TPU v7x, 512 devices: a 8x2x16 block of a 8x16x16 slice. The times are simulated.
512 devices in a mesh: grp: 2 (over y), sp: 16 (over z), tp: 16 (over x, core).
Axes of the slice: x: 8, y: 2, z: 16, core: 2. Of those that a mesh axis runs over, the one named last changes fastest.
The devices are a block of a 8x16x16 slice.
Arguments:
- hidden_in: bfloat16 [8192, 2048], P(('grp', 'sp'), 'tp'), parts along dimension 0, may hold values from -40 to 40
- norm_gain: float32 [3, 2048], replicated, may hold values from 0.1 to 1.9
- query_weight: bfloat16 [3, 1024, 2048], P(None, 'tp'), may hold values from -6 to 6
- key_weight: bfloat16 [3, 1024, 2048], P(None, 'tp'), may hold values from -6 to 6
- value_weight: bfloat16 [3, 1024, 2048], P(None, 'tp'), may hold values from -0.125 to 0.125
- output_weight: bfloat16 [3, 1024, 2048], P(None, None, 'tp'), may hold values from -0.75 to 0.75
- offset_bias: float32 [3, 16, 15, 31], P(None, 'tp'), may hold values from -4 to 4
Outputs:
- hidden_out: bfloat16 [8192, 2048], P(('grp', 'sp'), 'tp'), parts along dimension 0
There are 2 independent parts, one for each index of `grp`. A program takes and returns all parts, laid end to end along the dimension named above; an argument that names none is the same for every part. Nothing has to cross between parts.
All inputs are finite; a program needn't handle non-finite values.
Results may differ from a plain program's by a relative error of at most 0.028.
Values may be sent and summed in bfloat16 or wider, within the bound.
A program may use at most 64 MiB of HBM per device.

v0:
```python
from functools import partial

import jax
import jax.numpy as jnp
import numpy as np
from jax import lax
from jax.sharding import PartitionSpec as P

HEAD_DIM = 64
GRID_W = 64
ROW_SPAN = 8
COL_SPAN = 16
LAYERS = 3


EPS = 1e-06
NEG = -1e30
QBLOCK = 16


def from_everyone(array, axis):
    size = lax.axis_size(axis)
    return lax.all_to_all(
        jnp.broadcast_to(array[None], (size, *array.shape)), axis, 0, 0, tiled=True
    )


def in_order(blocks, dim):
    shape = list(blocks.shape[1:])
    shape[dim] *= blocks.shape[0]
    return jnp.moveaxis(blocks, 0, dim).reshape(shape)


def gather_directly(array, axis, dim):
    blocks = from_everyone(array, axis)
    return in_order(blocks, dim)


def padded(block, sides, width):
    for axis, dim in sides:
        count = lax.axis_size(axis)
        forward = [(i, i + 1) for i in range(count - 1)]
        backward = [(target, source) for source, target in forward]
        low = lax.ppermute(
            lax.slice_in_dim(block, block.shape[dim] - width, None, axis=dim), axis, forward
        )
        high = lax.ppermute(lax.slice_in_dim(block, 0, width, axis=dim), axis, backward)
        block = jnp.concatenate([low, block, high], axis=dim)
    return block


def column_tables():
    nblocks = GRID_W // QBLOCK
    key_span = QBLOCK + COL_SPAN
    block_start = np.clip(np.arange(nblocks) * QBLOCK - COL_SPAN // 2, 0, GRID_W - key_span)
    key_cols = block_start[:, None] + np.arange(key_span)[None, :]
    query_cols = np.arange(nblocks)[:, None] * QBLOCK + np.arange(QBLOCK)[None, :]
    window_cols = np.clip(query_cols - COL_SPAN // 2, 0, GRID_W - COL_SPAN)
    inside = (key_cols[:, None, :] >= window_cols[:, :, None]) & (
        key_cols[:, None, :] < window_cols[:, :, None] + COL_SPAN
    )
    col_offset = (
        np.clip(key_cols[:, None, :] - query_cols[:, :, None], 1 - COL_SPAN, COL_SPAN - 1)
        + COL_SPAN
        - 1
    )
    return (block_start, inside, col_offset)


def block_firsts():
    nblocks = GRID_W // QBLOCK
    key_span = QBLOCK + COL_SPAN
    return [
        min(max(block * QBLOCK - COL_SPAN // 2, 0), GRID_W - key_span) for block in range(nblocks)
    ]


def offset_bias_rows(bias_table, row_offset):
    block_start, inside, col_offset = column_tables()
    nblocks = block_start.shape[0]
    key_span = QBLOCK + COL_SPAN
    rows_n = row_offset.shape[0]
    heads_n = bias_table.shape[0]
    col_onehot = (np.arange(2 * COL_SPAN - 1)[:, None] == col_offset.reshape(1, -1)).astype(
        np.float32
    )
    by_col = jnp.einsum(
        "hjc,cm->hjm", bias_table, jnp.asarray(col_onehot), precision=lax.Precision.HIGHEST
    )
    row_onehot = (
        row_offset[:, :, None] == jnp.arange(2 * ROW_SPAN - 1, dtype=jnp.int32)[None, None, :]
    ).astype(jnp.float32)
    expanded = jnp.einsum("rsj,hjm->rhsm", row_onehot, by_col, precision=lax.Precision.HIGHEST)
    expanded = expanded.reshape(rows_n, heads_n, ROW_SPAN, nblocks, QBLOCK, key_span)
    return expanded.transpose(0, 1, 3, 4, 2, 5).reshape(
        rows_n, heads_n, nblocks, QBLOCK, ROW_SPAN * key_span
    )


def attend_rows(queries, key_rows, value_rows, bias):
    block_start, inside, col_offset = column_tables()
    nblocks = block_start.shape[0]
    key_span = QBLOCK + COL_SPAN
    rows_n, heads_n = (queries.shape[0], queries.shape[2])

    def pick_blocks(tensor):
        pieces = [tensor[:, :, first_col : first_col + key_span] for first_col in block_firsts()]
        return jnp.stack(pieces, axis=1).reshape(
            rows_n, nblocks, ROW_SPAN * key_span, heads_n, HEAD_DIM
        )

    key_blocks = pick_blocks(key_rows)
    value_blocks = pick_blocks(value_rows)
    query_blocks = queries.reshape(rows_n, nblocks, QBLOCK, heads_n, HEAD_DIM)
    scores = jnp.einsum(
        "rcqhd,rckhd->rhcqk", query_blocks, key_blocks, preferred_element_type=jnp.float32
    )
    scores = scores * HEAD_DIM ** (-0.5) + bias
    allowed = np.broadcast_to(inside[:, :, None, :], (nblocks, QBLOCK, ROW_SPAN, key_span))
    allowed = allowed.reshape(nblocks, QBLOCK, ROW_SPAN * key_span)
    scores = jnp.where(jnp.asarray(allowed)[None, None], scores, NEG)
    row_peak = jnp.max(scores, axis=-1, keepdims=True)
    lifted = jnp.exp(scores - row_peak)
    weights = (lifted / jnp.sum(lifted, axis=-1, keepdims=True)).astype(jnp.bfloat16)
    attended = jnp.einsum(
        "rhcqk,rckhd->rcqhd", weights, value_blocks, preferred_element_type=jnp.float32
    )
    return attended.astype(jnp.bfloat16).reshape(rows_n * GRID_W, heads_n * HEAD_DIM)


def contract(left, weight_rows):
    return lax.dot_general(
        left, weight_rows, (((1,), (1,)), ((), ())), preferred_element_type=jnp.float32
    )


def project(source, gain_row, query_w, key_w, value_w):
    gathered = gather_directly(source, "tp", 1)
    gathered_wide = gathered.astype(jnp.float32)
    row_scale = lax.rsqrt(jnp.mean(gathered_wide * gathered_wide, axis=1) + EPS)
    normed = (gathered_wide * row_scale[:, None] * gain_row[None, :]).astype(jnp.bfloat16)
    products = (contract(normed, query_w), contract(normed, key_w), contract(normed, value_w))
    return tuple((product.astype(jnp.bfloat16) for product in products))


def window_rows(pair_grid, first_index):
    return lax.dynamic_slice_in_dim(pair_grid, first_index, ROW_SPAN, 0)


def body(hidden_in, norm_gain, query_weight, key_weight, value_weight, output_weight, offset_bias):
    tok_dev, width_local = hidden_in.shape
    rows_dev = tok_dev // GRID_W
    span_half = ROW_SPAN // 2
    channels = query_weight.shape[1]
    heads_local = channels // HEAD_DIM
    all_rows = rows_dev * lax.axis_size("sp")
    first_row = lax.axis_index("sp") * rows_dev
    query_rows = first_row + jnp.arange(rows_dev, dtype=jnp.int32)
    window_first = jnp.clip(query_rows - span_half, 0, all_rows - ROW_SPAN)
    local_first = window_first - first_row + span_half
    row_offset = (
        window_first[:, None]
        + jnp.arange(ROW_SPAN, dtype=jnp.int32)[None, :]
        - query_rows[:, None]
        + ROW_SPAN
        - 1
    )
    stream = hidden_in
    for layer_idx in range(LAYERS):
        gain_row = norm_gain[layer_idx]
        queries, keys_made, values_made = project(
            stream,
            gain_row,
            query_weight[layer_idx],
            key_weight[layer_idx],
            value_weight[layer_idx],
        )
        pair_local = jnp.concatenate([keys_made, values_made], axis=1).reshape(
            rows_dev, GRID_W, 2 * channels
        )
        pair_grid = padded(pair_local, (("sp", 0),), span_half)
        picked = jax.vmap(partial(window_rows, pair_grid))(local_first)
        key_rows = picked[..., :channels].reshape(rows_dev, ROW_SPAN, GRID_W, heads_local, HEAD_DIM)
        value_rows = picked[..., channels:].reshape(
            rows_dev, ROW_SPAN, GRID_W, heads_local, HEAD_DIM
        )
        query_grid = queries.reshape(rows_dev, GRID_W, heads_local, HEAD_DIM)
        bias = offset_bias_rows(offset_bias[layer_idx], row_offset)
        attended = attend_rows(query_grid, key_rows, value_rows, bias)
        out_local = output_weight[layer_idx]
        projected = jnp.dot(
            gather_directly(attended, "tp", 1), out_local, preferred_element_type=jnp.float32
        )
        stream = (stream.astype(jnp.float32) + projected).astype(jnp.bfloat16)
    return stream


def solution(mesh):
    return jax.shard_map(
        body,
        mesh=mesh,
        in_specs=(
            P(("grp", "sp"), "tp"),
            P(),
            P(None, "tp", None),
            P(None, "tp", None),
            P(None, "tp", None),
            P(None, None, "tp"),
            P(None, "tp", None, None),
        ),
        out_specs=P(("grp", "sp"), "tp"),
        check_vma=False,
    )
```

profile of v0, /device:TPU:65, one launch (start us, length us, event | category | flops | bytes accessed | tf_op | source)
XLA Modules:
  0.0 251.0 jit_solution(13024179306977469757)
XLA Ops:
  0.0 0.9 copy.53
  0.9 1.1 broadcast_in_dim.42
  2.0 45.0 %all-to-all-start = ((bf16[16,256,128]{1,2,0:T(8,128)(2,1)}), bf16[16,256,128]{1,2,0:T(8,128)(2,1)S(1)}, u32[]{:S(2)}, u32[]{:S(2)}) async-start(bf16[16,256,128]{1,2,0:T(8,128)(2,1)} %broadcast_in_dim.42), calls=%async_computation | async-start | bytes 2097152 | tf_op jit(solution)/shard_map/all_to_all | solution.py:23
  47.1 0.6 fusion.116
  47.7 0.3 convolution_bitcast_fusion.5
  48.0 0.3 convolution_bitcast_fusion.2
  48.3 0.3 reshape.438
  48.7 0.6 copy.112
  49.3 1.0 reshape.439
  50.4 0.6 fusion.115
  51.0 24.2 %all-to-all-done = bf16[16,256,128]{1,2,0:T(8,128)(2,1)S(1)} async-done(((bf16[16,256,128]{1,2,0:T(8,128)(2,1)}), bf16[16,256,128]{1,2,0:T(8,128)(2,1)S(1)}, u32[]{:S(2)}, u32[]{:S(2)}) %all-to-all-start) | async-done | bytes 1048608 | tf_op jit(solution)/shard_map/all_to_all | solution.py:23
  75.2 0.3 fusion.3
  75.5 0.3 fusion.5
  75.9 1.3 convolution_convert_fusion.11
  77.1 1.3 convolution_convert_fusion.10
  78.5 1.3 collective-permute-start.1
  79.8 4.0 %collective-permute-start = (bf16[4,64,128]{2,1,0:T(8,128)(2,1)S(1)}, bf16[4,64,128]{2,1,0:T(8,128)(2,1)S(1)}, u32[]{:S(2)}, u32[]{:S(2)}) collective-permute-start(bf16[4,64,128]{2,1,0:T(8,128)(2,1)S(1)} %bitcast.261), channel_id=1, source_target_pairs={{0,16},{16,32},{32,48},{48,64},{64,80},{80,96},{96,112},{112,128},... | collective-permute-start | bytes 196616 | tf_op jit(solution)/shard_map/ppermute | solution.py:44
  83.8 1.2 convolution_convert_fusion.9
  85.3 0.7 gather_fusion
  85.9 0.2 slice_bitcast_fusion.4
  86.2 0.5 fusion.113
  87.2 0.4 copy-done.2
  88.5 0.5 convolution_convert_fusion.2
  89.2 21.5 %all_to_all.30 = bf16[16,256,64]{1,2,0:T(8,128)(2,1)S(1)} all-to-all(bf16[16,256,64]{1,2,0:T(8,128)(2,1)S(1)} %broadcast_in_dim.46), channel_id=1, replica_groups=mesh['grp'=2,'sp'=16,'tp'=16] {'tp'}, dimensions={0} | all-to-all | bytes 1048576 | tf_op jit(solution)/shard_map/all_to_all | solution.py:23
  110.7 1.3 fusion.24
  112.1 1.1 broadcast_in_dim.47
  113.2 3.9 %all-to-all-start.2 = ((bf16[16,256,128]{1,2,0:T(8,128)(2,1)}), bf16[16,256,128]{1,2,0:T(8,128)(2,1)S(1)}, u32[]{:S(2)}, u32[]{:S(2)}) async-start(bf16[16,256,128]{1,2,0:T(8,128)(2,1)} %broadcast_in_dim.47), calls=%async_computation.2 | async-start | bytes 2097152 | tf_op jit(solution)/shard_map/all_to_all | solution.py:23
  117.2 0.3 convolution_bitcast_fusion.4
  117.5 0.3 convolution_bitcast_fusion.1
  117.8 0.3 reshape.448
  118.1 0.6 copy.111
  118.7 1.0 reshape.449
  119.8 24.5 %all-to-all-done.2 = bf16[16,256,128]{1,2,0:T(8,128)(2,1)S(1)} async-done(((bf16[16,256,128]{1,2,0:T(8,128)(2,1)}), bf16[16,256,128]{1,2,0:T(8,128)(2,1)S(1)}, u32[]{:S(2)}, u32[]{:S(2)}) %all-to-all-start.2) | async-done | bytes 1048608 | tf_op jit(solution)/shard_map/all_to_all | solution.py:23
  144.3 0.3 fusion.6
  144.6 0.3 fusion.8
  144.9 1.3 convolution_convert_fusion.8
  146.2 1.3 convolution_convert_fusion.7
  147.6 1.3 collective-permute-start.3
  148.9 4.8 %collective-permute-start.2 = (bf16[4,64,128]{2,1,0:T(8,128)(2,1)S(1)}, bf16[4,64,128]{2,1,0:T(8,128)(2,1)S(1)}, u32[]{:S(2)}, u32[]{:S(2)}) collective-permute-start(bf16[4,64,128]{2,1,0:T(8,128)(2,1)S(1)} %bitcast.264), channel_id=1, source_target_pairs={{0,16},{16,32},{32,48},{48,64},{64,80},{80,96},{96,112},{112,128},... | collective-permute-start | bytes 196616 | tf_op jit(solution)/shard_map/ppermute | solution.py:44
  153.7 1.2 convolution_convert_fusion.6
  155.2 0.7 gather_fusion.1
  156.8 0.4 copy-done.3
  158.3 0.5 convolution_convert_fusion.1
  159.0 21.1 %all_to_all.31 = bf16[16,256,64]{1,2,0:T(8,128)(2,1)S(1)} all-to-all(bf16[16,256,64]{1,2,0:T(8,128)(2,1)S(1)} %broadcast_in_dim.50), channel_id=1, replica_groups=mesh['grp'=2,'sp'=16,'tp'=16] {'tp'}, dimensions={0} | all-to-all | bytes 1048576 | tf_op jit(solution)/shard_map/all_to_all | solution.py:23
  180.1 1.3 fusion.25
  181.5 1.1 broadcast_in_dim.51
  182.6 3.8 %all-to-all-start.4 = ((bf16[16,256,128]{1,2,0:T(8,128)(2,1)}), bf16[16,256,128]{1,2,0:T(8,128)(2,1)S(1)}, u32[]{:S(2)}, u32[]{:S(2)}) async-start(bf16[16,256,128]{1,2,0:T(8,128)(2,1)} %broadcast_in_dim.51), calls=%async_computation.4 | async-start | bytes 2097152 | tf_op jit(solution)/shard_map/all_to_all | solution.py:23
  186.4 0.3 convolution_bitcast_fusion.3
  186.7 0.3 convolution_bitcast_fusion
  187.0 0.3 reshape.458
  187.3 0.6 copy.110
  188.0 0.3 reshape.459
  188.3 25.2 %all-to-all-done.4 = bf16[16,256,128]{1,2,0:T(8,128)(2,1)S(1)} async-done(((bf16[16,256,128]{1,2,0:T(8,128)(2,1)}), bf16[16,256,128]{1,2,0:T(8,128)(2,1)S(1)}, u32[]{:S(2)}, u32[]{:S(2)}) %all-to-all-start.4) | async-done | bytes 1048608 | tf_op jit(solution)/shard_map/all_to_all | solution.py:23
  213.5 0.3 fusion.9
  213.8 0.3 fusion.11
  214.2 1.2 convolution_convert_fusion.5
  215.4 1.3 convolution_convert_fusion.4
  216.8 1.3 collective-permute-start.5
  218.1 4.7 %collective-permute-start.4 = (bf16[4,64,128]{2,1,0:T(8,128)(2,1)S(1)}, bf16[4,64,128]{2,1,0:T(8,128)(2,1)S(1)}, u32[]{:S(2)}, u32[]{:S(2)}) collective-permute-start(bf16[4,64,128]{2,1,0:T(8,128)(2,1)S(1)} %bitcast.267), channel_id=1, source_target_pairs={{0,16},{16,32},{32,48},{48,64},{64,80},{80,96},{96,112},{112,128},... | collective-permute-start | bytes 196616 | tf_op jit(solution)/shard_map/ppermute | solution.py:44
  222.8 1.2 convolution_convert_fusion.3
  224.2 0.7 gather_fusion.2
  227.1 0.5 convolution_convert_fusion
  227.8 21.3 %all_to_all.32 = bf16[16,256,64]{1,2,0:T(8,128)(2,1)S(1)} all-to-all(bf16[16,256,64]{1,2,0:T(8,128)(2,1)S(1)} %broadcast_in_dim.99), channel_id=1, replica_groups=mesh['grp'=2,'sp'=16,'tp'=16] {'tp'}, dimensions={0} | all-to-all | bytes 1048576 | tf_op jit(solution)/shard_map/all_to_all | solution.py:23
  249.1 1.9 fusion.26
  (90 shorter events, 7.2 us)
Async XLA Ops:
  2.0 45.0 %copy-start.7 = (f32[3,1,15,31]{3,1,2,0:T(1,128)S(1)}, f32[3,1,15,31]{3,1,2,0:T(1,128)}, u32[]{:S(2)}) copy-start(f32[3,1,15,31]{3,1,2,0:T(1,128)} %param.19) | copy-start | bytes 16744
  2.0 45.6 %copy-start = (f32[31,2048]{1,0:T(8,128)S(1)}, f32[31,2048]{1,0:T(8,128)}, u32[]{:S(2)}) copy-start(f32[31,2048]{1,0:T(8,128)} %constant.43.clone) | copy-start | bytes 761860
  2.0 73.1 %all-to-all-start = ((bf16[16,256,128]{1,2,0:T(8,128)(2,1)}), bf16[16,256,128]{1,2,0:T(8,128)(2,1)S(1)}, u32[]{:S(2)}, u32[]{:S(2)}) async-start(bf16[16,256,128]{1,2,0:T(8,128)(2,1)} %broadcast_in_dim.42), calls=%async_computation | async-start | bytes 2097152 | tf_op jit(solution)/shard_map/all_to_all | solution.py:23
  49.3 1.1 copy-start.8
  78.5 6.7 %collective-permute-start.1 = (bf16[4,64,128]{2,1,0:T(8,128)(2,1)S(1)}, bf16[4,64,128]{2,1,0:T(8,128)(2,1)S(1)}, u32[]{:S(2)}, u32[]{:S(2)}) collective-permute-start(bf16[4,64,128]{2,1,0:T(8,128)(2,1)S(1)} %bitcast.260), channel_id=1, source_target_pairs={{16,0},{32,16},{48,32},{64,48},{80,64},{96,80},{112,96},{128,112},... | collective-permute-start | bytes 196616 | tf_op jit(solution)/shard_map/ppermute | solution.py:47
  79.8 5.4 %collective-permute-start = (bf16[4,64,128]{2,1,0:T(8,128)(2,1)S(1)}, bf16[4,64,128]{2,1,0:T(8,128)(2,1)S(1)}, u32[]{:S(2)}, u32[]{:S(2)}) collective-permute-start(bf16[4,64,128]{2,1,0:T(8,128)(2,1)S(1)} %bitcast.261), channel_id=1, source_target_pairs={{0,16},{16,32},{32,48},{48,64},{64,80},{80,96},{96,112},{112,128},... | collective-permute-start | bytes 196616 | tf_op jit(solution)/shard_map/ppermute | solution.py:44
  86.6 1.0 copy-start.2
  86.7 0.9 copy-start.9
  89.0 21.7 %copy-start.1 = (bf16[256,128]{1,0:T(8,128)(2,1)S(1)}, bf16[256,128]{1,0:T(8,128)(2,1)}, u32[]{:S(2)}) copy-start(bf16[256,128]{1,0:T(8,128)(2,1)} %param.13) | copy-start | bytes 196612
  113.2 4.0 %copy-start.4 = (f32[1,1,15,31]{3,1,2,0:T(1,128)S(1)}, f32[1,1,15,31]{3,1,2,0:T(1,128)}, u32[]{:S(2)}) copy-start(f32[1,1,15,31]{3,1,2,0:T(1,128)} %get-tuple-element.40) | copy-start | bytes 5584
  113.2 31.1 %all-to-all-start.2 = ((bf16[16,256,128]{1,2,0:T(8,128)(2,1)}), bf16[16,256,128]{1,2,0:T(8,128)(2,1)S(1)}, u32[]{:S(2)}, u32[]{:S(2)}) async-start(bf16[16,256,128]{1,2,0:T(8,128)(2,1)} %broadcast_in_dim.47), calls=%async_computation.2 | async-start | bytes 2097152 | tf_op jit(solution)/shard_map/all_to_all | solution.py:23
  118.7 25.9 %copy-start.6 = (f32[1,2048]{1,0:T(1,128)S(1)}, f32[1,2048]{1,0:T(1,128)}, u32[]{:S(2)}) copy-start(f32[1,2048]{1,0:T(1,128)} %get-tuple-element.37) | copy-start | bytes 24580
  147.6 7.5 %collective-permute-start.3 = (bf16[4,64,128]{2,1,0:T(8,128)(2,1)S(1)}, bf16[4,64,128]{2,1,0:T(8,128)(2,1)S(1)}, u32[]{:S(2)}, u32[]{:S(2)}) collective-permute-start(bf16[4,64,128]{2,1,0:T(8,128)(2,1)S(1)} %bitcast.263), channel_id=1, source_target_pairs={{16,0},{32,16},{48,32},{64,48},{80,64},{96,80},{112,96},{128,112},... | collective-permute-start | bytes 196616 | tf_op jit(solution)/shard_map/ppermute | solution.py:47
  148.9 6.2 %collective-permute-start.2 = (bf16[4,64,128]{2,1,0:T(8,128)(2,1)S(1)}, bf16[4,64,128]{2,1,0:T(8,128)(2,1)S(1)}, u32[]{:S(2)}, u32[]{:S(2)}) collective-permute-start(bf16[4,64,128]{2,1,0:T(8,128)(2,1)S(1)} %bitcast.264), channel_id=1, source_target_pairs={{0,16},{16,32},{32,48},{48,64},{64,80},{80,96},{96,112},{112,128},... | collective-permute-start | bytes 196616 | tf_op jit(solution)/shard_map/ppermute | solution.py:44
  156.2 1.0 copy-start.3
  156.3 0.9 copy-start.10
  182.6 30.9 %all-to-all-start.4 = ((bf16[16,256,128]{1,2,0:T(8,128)(2,1)}), bf16[16,256,128]{1,2,0:T(8,128)(2,1)S(1)}, u32[]{:S(2)}, u32[]{:S(2)}) async-start(bf16[16,256,128]{1,2,0:T(8,128)(2,1)} %broadcast_in_dim.51), calls=%async_computation.4 | async-start | bytes 2097152 | tf_op jit(solution)/shard_map/all_to_all | solution.py:23
  187.9 25.9 %copy-start.5 = (f32[1,2048]{1,0:T(1,128)S(1)}, f32[1,2048]{1,0:T(1,128)}, u32[]{:S(2)}) copy-start(f32[1,2048]{1,0:T(1,128)} %get-tuple-element.35) | copy-start | bytes 24580
  216.8 7.4 %collective-permute-start.5 = (bf16[4,64,128]{2,1,0:T(8,128)(2,1)S(1)}, bf16[4,64,128]{2,1,0:T(8,128)(2,1)S(1)}, u32[]{:S(2)}, u32[]{:S(2)}) collective-permute-start(bf16[4,64,128]{2,1,0:T(8,128)(2,1)S(1)} %bitcast.266), channel_id=1, source_target_pairs={{16,0},{32,16},{48,32},{64,48},{80,64},{96,80},{112,96},{128,112},... | collective-permute-start | bytes 196616 | tf_op jit(solution)/shard_map/ppermute | solution.py:47
  218.1 6.0 %collective-permute-start.4 = (bf16[4,64,128]{2,1,0:T(8,128)(2,1)S(1)}, bf16[4,64,128]{2,1,0:T(8,128)(2,1)S(1)}, u32[]{:S(2)}, u32[]{:S(2)}) collective-permute-start(bf16[4,64,128]{2,1,0:T(8,128)(2,1)S(1)} %bitcast.267), channel_id=1, source_target_pairs={{0,16},{16,32},{32,48},{48,64},{64,80},{80,96},{96,112},{112,128},... | collective-permute-start | bytes 196616 | tf_op jit(solution)/shard_map/ppermute | solution.py:44
  225.3 0.7 copy-start.11
where the time goes:
time: 252 us; the launch traced here: 251 us
  waiting for transfers between devices  73.9 us (29%)
  starting transfers between devices  70.2 us (28%)
  blocking collectives  63.9 us (25%)
  local copies, waits for them, and re-layouts  19.9 us (8%)
  matrix products  19.5 us (8%)
  other arithmetic  2.76 us (1%)
    all_to_all x3, waiting for transfers between devices, from_everyone(): lax.all_to_all(jnp.broadcast_to(array[None], (size, *array.shape)), axis,...  73.9 us
    all_to_all x3, blocking collectives, from_everyone(): lax.all_to_all(jnp.broadcast_to(array[None], (size, *array.shape)), axis,...  63.9 us
    all_to_all x3, starting transfers between devices, from_everyone(): lax.all_to_all(jnp.broadcast_to(array[None], (size, *array.shape)), axis,...  52.8 us
    ppermute x3, starting transfers between devices, padded(): lax.ppermute(lax.slice_in_dim(block, block.shape[dim] - width, None, axis...  13.5 us
    dot_general x9, matrix products, contract(): lax.dot_general(left, weight_rows, (((1,), (1,)), ((), ())), preferred_el...  11.2 us
  transfers between devices with their start and end apart: 9, of which 3 were waited for; matrix products, arithmetic and copies ran while one was open for 5% of the time, Pallas kernels for 0%

commit v1 on v0

v1 whole, which is shorter than its diff:
```python
import functools

import jax
import jax.numpy as jnp
from jax import lax
from jax.experimental import pallas as pl
from jax.experimental.pallas import tpu as pltpu
from jax.sharding import PartitionSpec as P

HEAD_DIM = 64
GRID_W = 64
ROW_SPAN = 8
COL_SPAN = 16
EPS = 1e-06
NEG = -1e30
MESH = pl.DeviceIdType.MESH
ORDER = (4, 3, 5, 2, 6, 1, 7)
ARRIVE = (1, 7, 2, 6, 3, 5, 4)


def kernel(
    n_sp,
    n_tp,
    layers,
    hid_ref,
    gain_ref,
    wq_ref,
    wk_ref,
    wv_ref,
    wo_ref,
    ob_ref,
    out_ref,
    xst,
    last_half,
    xs,
    atts,
    kv,
    wraw,
    wg,
    wout,
    tab,
    bias,
    own_w_sem,
    own_o_sem,
    own_x_sem,
    d2d_s,
    d2d_r,
    x_s,
    x_r,
    a_s,
    a_r,
    h_s,
    h_r,
):
    chips = n_tp // 2
    tok = xs.shape[2]
    feat = xs.shape[3]
    half = feat // 2
    tp = lax.axis_index("tp")
    sp = lax.axis_index("sp")
    core = lax.rem(tp, 2)
    chip = lax.div(tp, 2)
    mate = tp + 1 - 2 * core
    up = lax.rem(sp + 1, n_sp)
    down = lax.rem(sp + n_sp - 1, n_sp)

    def peer(j):
        return {"tp": lax.rem(tp + 2 * j, n_tp)}

    def rows_at(start, size, align):
        return pl.ds(pl.multiple_of(start, align), size)

    greet = [peer(j) for j in range(1, chips)]
    greet += [{"tp": mate}]
    greet += [{"sp": z, "tp": t} for z in (up, down) for t in (tp, mate)]
    barrier = pltpu.get_barrier_semaphore()
    for device in greet:
        pl.semaphore_signal(barrier, inc=1, device_id=device, device_id_type=MESH)

    my_lanes = rows_at(core * half, half, half)
    own_x = [
        pltpu.make_async_copy(
            hid_ref.at[rows_at((1 - core) * tok, tok, tok), :], xst, own_x_sem.at[0]
        ),
        pltpu.make_async_copy(
            hid_ref.at[rows_at(core * tok, tok, tok), :], xs.at[0, 0, :, my_lanes], own_x_sem.at[1]
        ),
    ]
    for copy in own_x:
        copy.start()
    w_rows = (
        rows_at(HEAD_DIM * (1 - core), HEAD_DIM, HEAD_DIM),
        rows_at(192 + 64 * core, HEAD_DIM, HEAD_DIM),
        rows_at(128 + 192 * core, HEAD_DIM, HEAD_DIM),
    )
    own_w = []
    own_o = []
    for layer in range(layers):
        for i, w_ref in enumerate((wq_ref, wk_ref, wv_ref)):
            copy = pltpu.make_async_copy(
                w_ref.at[layer], wraw.at[layer, w_rows[i], :], own_w_sem.at[layer, i]
            )
            copy.start()
            own_w.append(copy)
    for layer in range(layers):
        copy = pltpu.make_async_copy(
            wo_ref.at[layer], wout.at[layer, :, my_lanes], own_o_sem.at[layer]
        )
        copy.start()
        own_o.append(copy)

    tab[1] = jnp.zeros(tab.shape[1:], jnp.float32)
    for layer in range(layers):
        tab[1, layer, 0:15, 0:31] = ob_ref[layer]
    for layer in range(layers):
        raw = tab[1, layer]
        low = pltpu.roll(raw, 128 - 15, 1)
        high = pltpu.roll(pltpu.roll(raw, 64 - 15, 1), 15, 0)
        tab[0, layer] = low + high

    pl.semaphore_wait(barrier, len(greet))

    sends = []

    def send(src, dst, s_sem, r_sem, device):
        copy = pltpu.make_async_remote_copy(
            src_ref=src,
            dst_ref=dst,
            send_sem=s_sem,
            recv_sem=r_sem,
            device_id=device,
            device_id_type=MESH,
        )
        copy.start()
        sends.append(copy)
        return copy

    own_x[0].wait()
    x_mate = send(xst, xs.at[0, 0, :, my_lanes], d2d_s.at[0], d2d_r.at[0], {"tp": mate})
    w_mate = []
    sem = 2
    for layer in range(layers):
        for i, w_ref in enumerate((wq_ref, wk_ref, wv_ref)):
            w_mate.append(
                send(
                    w_ref.at[layer],
                    wraw.at[layer, w_rows[i], :],
                    d2d_s.at[sem],
                    d2d_r.at[sem],
                    {"tp": mate},
                )
            )
            sem += 1
        if layer == 0:
            own_x[1].wait()
            x_mate.wait_recv()
            x_gather = [None] * chips
            for j in ORDER:
                x_gather[j] = send(xs.at[0, 0], xs.at[0, j], x_s.at[0, j], x_r.at[0, j], peer(j))
            t_mate = send(tab.at[0], tab.at[2], d2d_s.at[1], d2d_r.at[1], {"tp": mate})
    o_mate = []
    for layer in range(layers):
        o_mate.append(
            send(
                wo_ref.at[layer],
                wout.at[layer, :, my_lanes],
                d2d_s.at[sem],
                d2d_r.at[sem],
                {"tp": mate},
            )
        )
        sem += 1

    def scale_layer(layer):
        for copy in own_w[3 * layer : 3 * layer + 3]:
            copy.wait()
        for copy in w_mate[3 * layer : 3 * layer + 3]:
            copy.wait_recv()

        def one(j, carry):
            source = lax.rem(chip - j + chips, chips)
            lanes = rows_at(source * feat, feat, feat)
            gain = gain_ref[pl.ds(layer, 1), lanes]
            scale = HEAD_DIM ** (-0.5)
            wg[layer, j, 0:128, :] = (
                wraw[layer, 0:128, lanes].astype(jnp.float32) * (gain * scale)
            ).astype(jnp.bfloat16)
            wg[layer, j, 128:384, :] = (
                wraw[layer, 128:384, lanes].astype(jnp.float32) * gain
            ).astype(jnp.bfloat16)
            return carry

        lax.fori_loop(0, chips, one, 0)

    all_rows = n_sp * 4
    starts = []
    offsets = []
    for i in range(2):
        row = sp * 4 + core * 2 + i
        first = jnp.clip(row - ROW_SPAN // 2, 0, all_rows - ROW_SPAN)
        starts.append(first - sp * 4 + 4)
        offsets.append(first - row + ROW_SPAN - 1)

    def make_bias():
        t_mate.wait_recv()
        lane = lax.broadcasted_iota(jnp.int32, (GRID_W, 128), 1)
        key_col = jnp.where(lane < GRID_W, lane, lane - GRID_W)
        query_col = lax.broadcasted_iota(jnp.int32, (GRID_W, 128), 0)
        window = jnp.clip(query_col - COL_SPAN // 2, 0, GRID_W - COL_SPAN)
        inside = (key_col >= window) & (key_col < window + COL_SPAN)

        def one(layer, carry):
            for head in range(2):
                which = jnp.where(core == head, 0, 2)
                for i in range(2):
                    for pair in range(4):
                        line = tab[which, layer, pl.ds(offsets[i] + 2 * pair, 1), :]
                        wide = jnp.broadcast_to(line, (GRID_W, 128))
                        rolled = pltpu.roll(wide, 0, 1, stride=1, stride_axis=0)
                        bias[layer, head, i, :, 128 * pair : 128 * pair + 128] = jnp.where(
                            inside, rolled, NEG
                        )
            return carry

        lax.fori_loop(0, layers, one, 0)

    scale_layer(0)
    make_bias()

    my_rows = rows_at(256 + core * tok, tok, tok)
    lane_low = lax.broadcasted_iota(jnp.int32, (GRID_W, 128), 1) < HEAD_DIM

    for layer in range(layers):
        made = None
        squares = None
        for j in (0,) + ARRIVE:
            if j:
                x_gather[j].wait_recv()
            block = xs[layer, j]
            wide = block.astype(jnp.float32)
            square = wide * wide
            part = lax.dot_general(
                block, wg[layer, j], (((1,), (1,)), ((), ())), preferred_element_type=jnp.float32
            )
            made = part if made is None else made + part
            squares = square if squares is None else squares + square
        mean = jnp.sum(squares, axis=1, keepdims=True) * (1.0 / (feat * chips))
        normed = made * lax.rsqrt(mean + EPS)
        queries = normed[:, 0:128].astype(jnp.bfloat16)
        kv[layer, my_rows, :] = normed[:, 128:384].astype(jnp.bfloat16)
        mine = kv.at[layer, my_rows, :]
        halo = [send(mine, mine, h_s.at[layer, 0], h_r.at[layer, 0], {"tp": mate})]
        above = kv.at[layer, rows_at(core * tok, tok, tok), :]
        below = kv.at[layer, rows_at(512 + core * tok, tok, tok), :]
        spots = ((above, up, tp), (below, down, tp), (above, up, mate), (below, down, mate))
        for i, (spot, z, t) in enumerate(spots):
            halo.append(
                send(mine, spot, h_s.at[layer, i + 1], h_r.at[layer, i + 1], {"sp": z, "tp": t})
            )
        if layer == 0:
            for other in range(1, layers):
                scale_layer(other)
        for copy in halo:
            copy.wait_recv()

        for i in range(2):
            outs = []
            for head in range(2):
                pick = lane_low if head == 1 else jnp.logical_not(lane_low)
                query = jnp.where(pick, queries[GRID_W * i : GRID_W * (i + 1)], 0)
                pairs = kv[
                    layer,
                    rows_at(starts[i] * GRID_W, ROW_SPAN * GRID_W, GRID_W),
                    128 * head : 128 * head + 128,
                ]
                scores = lax.dot_general(
                    query, pairs, (((1,), (1,)), ((), ())), preferred_element_type=jnp.float32
                )
                scores = scores + bias[layer, head, i]
                peak = jnp.max(scores, axis=1, keepdims=True)
                lifted = jnp.exp(scores - peak)
                total = jnp.sum(lifted, axis=1, keepdims=True)
                mixed = jnp.dot(
                    lifted.astype(jnp.bfloat16), pairs, preferred_element_type=jnp.float32
                )
                outs.append(mixed / total)
            both = jnp.where(lane_low, outs[0], outs[1])
            atts[layer, 0, GRID_W * i : GRID_W * (i + 1), :] = both.astype(jnp.bfloat16)

        gather = [None] * chips
        for j in ORDER:
            gather[j] = send(
                atts.at[layer, 0], atts.at[layer, j], a_s.at[layer, j], a_r.at[layer, j], peer(j)
            )
        own_o[layer].wait()
        o_mate[layer].wait_recv()
        stream = xs[layer, 0].astype(jnp.float32)
        for j in (0,) + ARRIVE:
            if j:
                gather[j].wait_recv()
            source = lax.rem(chip - j + chips, chips)
            stream = stream + jnp.dot(
                atts[layer, j],
                wout[layer, rows_at(source * 128, 128, 128), :],
                preferred_element_type=jnp.float32,
            )
        if layer + 1 < layers:
            xs[layer + 1, 0] = stream.astype(jnp.bfloat16)
            for j in ORDER:
                x_gather[j] = send(
                    xs.at[layer + 1, 0],
                    xs.at[layer + 1, j],
                    x_s.at[layer + 1, j],
                    x_r.at[layer + 1, j],
                    peer(j),
                )
        else:
            final = stream.astype(jnp.bfloat16)
            swap = core == 0
            keep = jnp.where(swap, final[:, 0:half], final[:, half:feat])
            last_half[...] = jnp.where(swap, final[:, half:feat], final[:, 0:half])
            place = rows_at(core * tok, tok, tok)
            last = send(last_half, out_ref.at[place, :], d2d_s.at[sem], d2d_r.at[sem], {"tp": mate})
            out_ref[place, :] = keep
            last.wait_recv()
    for copy in sends:
        copy.wait_send()


def body(hidden_in, norm_gain, query_weight, key_weight, value_weight, output_weight, offset_bias):
    n_sp = lax.axis_size("sp")
    n_tp = lax.axis_size("tp")
    chips = n_tp // 2
    layers = norm_gain.shape[0]
    width = norm_gain.shape[1]
    tokens, _ = hidden_in.shape
    tok = tokens // 2
    feat = width // chips
    any_space = pl.BlockSpec(memory_space=pl.ANY)
    vmem = pl.BlockSpec(memory_space=pltpu.VMEM)
    dma = pltpu.SemaphoreType.DMA
    bf16 = jnp.bfloat16
    table = offset_bias.reshape(layers, 2 * ROW_SPAN - 1, 2 * COL_SPAN - 1)
    return pl.pallas_call(
        functools.partial(kernel, n_sp, n_tp, layers),
        out_shape=jax.ShapeDtypeStruct(hidden_in.shape, bf16),
        in_specs=[any_space, vmem, any_space, any_space, any_space, any_space, vmem],
        out_specs=vmem,
        scratch_shapes=[
            pltpu.VMEM((tok, feat // 2), bf16),
            pltpu.VMEM((tok, feat // 2), bf16),
            pltpu.VMEM((layers, chips, tok, feat), bf16),
            pltpu.VMEM((layers, chips, tok, 128), bf16),
            pltpu.VMEM((layers, 768, 256), bf16),
            pltpu.VMEM((layers, 384, width), bf16),
            pltpu.VMEM((layers, chips, 384, feat), bf16),
            pltpu.VMEM((layers, 1024, feat), bf16),
            pltpu.VMEM((3, layers, 16, 128), jnp.float32),
            pltpu.VMEM((layers, 2, 2, GRID_W, ROW_SPAN * GRID_W), jnp.float32),
            dma((layers, 3)),
            dma((layers,)),
            dma((2,)),
            dma((3 + 4 * layers,)),
            dma((3 + 4 * layers,)),
            dma((layers, chips)),
            dma((layers, chips)),
            dma((layers, chips)),
            dma((layers, chips)),
            dma((layers, 5)),
            dma((layers, 5)),
        ],
        compiler_params=pltpu.CompilerParams(
            collective_id=0, has_side_effects=True, vmem_limit_bytes=48 * 1024 * 1024
        ),
        name="layers",
    )(hidden_in, norm_gain, query_weight, key_weight, value_weight, output_weight, table)


def solution(mesh):
    return jax.shard_map(
        body,
        mesh=mesh,
        in_specs=(
            P(("grp", "sp"), "tp"),
            P(),
            P(None, "tp", None),
            P(None, "tp", None),
            P(None, "tp", None),
            P(None, None, "tp"),
            P(None, "tp", None, None),
        ),
        out_specs=P(("grp", "sp"), "tp"),
        check_vma=False,
    )
```

time: 252 us -> 146 us (0.58)
  Pallas kernels: 0 us -> 138 us
  waiting for transfers between devices: 73.9 us -> 0 us
  starting transfers between devices: 70.2 us -> 0 us
  blocking collectives: 63.9 us -> 0 us
  matrix products: 19.5 us -> 0 us
  local copies, waits for them, and re-layouts: 19.9 us -> 6.77 us
  other arithmetic: 2.76 us -> 0 us
    pallas_call x0 -> x1, Pallas kernels: none -> 138 us  [body(): pl.pallas_call(functools.partial(kernel, n_sp, n_tp, layers), out_shape=j...]
    all_to_all x3 -> x0, waiting for transfers between devices: 73.9 us -> none  [from_everyone(): lax.all_to_all(jnp.broadcast_to(array[None], (size, *array.shape)), axis,...]
    all_to_all x3 -> x0, blocking collectives: 63.9 us -> none  [from_everyone(): lax.all_to_all(jnp.broadcast_to(array[None], (size, *array.shape)), axis,...]
    all_to_all x3 -> x0, starting transfers between devices: 52.8 us -> none  [from_everyone(): lax.all_to_all(jnp.broadcast_to(array[None], (size, *array.shape)), axis,...]
    dot_general x24 -> x0, matrix products: 19.5 us -> none  [the longest x9 11.2 us: contract(): lax.dot_general(left, weight_rows, (((1,), (1,)), ((), ())), preferred_el...]
    ppermute x6 -> x0, starting transfers between devices: 17.5 us -> none  [the longest x3 13.5 us: padded(): lax.ppermute(lax.slice_in_dim(block, block.shape[dim] - width, None, axis...]
    reshape x12 -> x0, local copies, waits for them, and re-layouts: 5.95 us -> none  [the longest x6 2.85 us: offset_bias_rows(): expanded.reshape(rows_n, heads_n, ROW_SPAN, nblocks, QBLOCK, key_span)]
    unnamed x25 -> x14, local copies, waits for them, and re-layouts: 1.94 us -> 6.77 us
  transfers between devices with their start and end apart: 9 -> 0, of which waited for: 3 -> 0; matrix products, arithmetic and copies ran while one was open for 5% -> 0% of each run, Pallas kernels for 0% -> 0%
where the time goes in v1:
time: 146 us; the launch traced here: 145 us
  Pallas kernels  138 us (95%)
  local copies, waits for them, and re-layouts  6.77 us (5%)
    pallas_call x1, Pallas kernels, body(): pl.pallas_call(functools.partial(kernel, n_sp, n_tp, layers), out_shape=j...  138 us
    unnamed x14, local copies, waits for them, and re-layouts  6.77 us

profile of v1, /device:TPU:65, one launch (start us, length us, event | category | flops | bytes accessed | tf_op | source)
XLA Modules:
  0.0 145.1 jit_solution(14719375956511120991)
XLA Ops:
  0.0 0.0 copy-start.5
  0.0 0.7 copy.10
  0.7 0.0 copy-done.5
  0.8 0.0 copy-start
  0.8 1.1 copy-done
  1.9 0.0 copy-start.1
  1.9 1.1 copy-done.1
  3.0 0.0 copy-start.2
  3.0 1.1 copy-done.2
  4.2 0.0 copy-start.3
  4.2 1.1 copy-done.3
  5.3 0.0 copy-start.4
  5.3 0.8 copy-done.4
  6.1 138.4 %layers.1 = bf16[256,128]{1,0:T(8,128)(2,1)S(1)} custom-call(bf16[256,128]{1,0:T(8,128)(2,1)S(1)} %copy-done.4, f32[3,2048]{1,0:T(4,128)S(1)} %copy-done.5, bf16[3,64,2048]{2,1,0:T(8,128)(2,1)S(1)} %copy-done, bf16[3,64,2048]{2,1,0:T(8,128)(2,1)S(1)} %copy-done.1, bf16[3,64,2048]{2,1,0:T(8,128)(2,1)S(1)} %copy-done.2, bf16[3,1024,128]{2,1,0:T(8,128)(2,1)S(1)} %copy-done.3, ...), custom_call_target="tpu_custom_call" | custom-call | tf_op jit(solution)/shard_map/layers/pallas_call | solution.py:344
  144.5 0.6 copy.12
Async XLA Ops:
  0.0 0.8 copy-start.5
  0.8 1.1 copy-start
  1.9 1.1 copy-start.1
  3.0 1.1 copy-start.2
  4.2 1.1 copy-start.3
  5.3 0.8 copy-start.4

commit v2 on v1

--- a/solution.py
+++ b/solution.py
@@ -23,13 +23,15 @@
     n_tp,
     layers,
     hid_ref,
-    gain_ref,
+    gain_hbm,
     wq_ref,
     wk_ref,
     wv_ref,
     wo_ref,
+    ob_hbm,
+    out_ref,
+    gain_ref,
     ob_ref,
-    out_ref,
     xst,
     last_half,
     xs,
@@ -86,7 +88,9 @@
             hid_ref.at[rows_at(core * tok, tok, tok), :], xs.at[0, 0, :, my_lanes], own_x_sem.at[1]
         ),
     ]
-    for copy in own_x:
+    own_g = pltpu.make_async_copy(gain_hbm, gain_ref, own_x_sem.at[2])
+    own_b = pltpu.make_async_copy(ob_hbm, ob_ref, own_x_sem.at[3])
+    for copy in own_x + [own_b, own_g]:
         copy.start()
     w_rows = (
         rows_at(HEAD_DIM * (1 - core), HEAD_DIM, HEAD_DIM),
@@ -110,8 +114,10 @@
         own_o.append(copy)
 
     tab[1] = jnp.zeros(tab.shape[1:], jnp.float32)
-    for layer in range(layers):
-        tab[1, layer, 0:15, 0:31] = ob_ref[layer]
+    own_b.wait()
+    for layer in range(layers):
+        for line in range(2 * ROW_SPAN - 1):
+            tab[1, layer, line : line + 1, 0:31] = ob_ref[layer, line]
     for layer in range(layers):
         raw = tab[1, layer]
         low = pltpu.roll(raw, 128 - 15, 1)
@@ -224,8 +230,10 @@
 
         lax.fori_loop(0, layers, one, 0)
 
+    own_g.wait()
     scale_layer(0)
     make_bias()
+    scale_layer(1)
 
     my_rows = rows_at(256 + core * tok, tok, tok)
     lane_low = lax.broadcasted_iota(jnp.int32, (GRID_W, 128), 1) < HEAD_DIM
@@ -258,7 +266,7 @@
                 send(mine, spot, h_s.at[layer, i + 1], h_r.at[layer, i + 1], {"sp": z, "tp": t})
             )
         if layer == 0:
-            for other in range(1, layers):
+            for other in range(2, layers):
                 scale_layer(other)
         for copy in halo:
             copy.wait_recv()
@@ -336,17 +344,19 @@
     tokens, _ = hidden_in.shape
     tok = tokens // 2
     feat = width // chips
-    any_space = pl.BlockSpec(memory_space=pl.ANY)
+    any_space = pl.BlockSpec(memory_space=pltpu.HBM)
     vmem = pl.BlockSpec(memory_space=pltpu.VMEM)
     dma = pltpu.SemaphoreType.DMA
     bf16 = jnp.bfloat16
-    table = offset_bias.reshape(layers, 2 * ROW_SPAN - 1, 2 * COL_SPAN - 1)
+    table = offset_bias.transpose(0, 2, 1, 3)
     return pl.pallas_call(
         functools.partial(kernel, n_sp, n_tp, layers),
         out_shape=jax.ShapeDtypeStruct(hidden_in.shape, bf16),
-        in_specs=[any_space, vmem, any_space, any_space, any_space, any_space, vmem],
+        in_specs=[any_space] * 7,
         out_specs=vmem,
         scratch_shapes=[
+            pltpu.VMEM(norm_gain.shape, jnp.float32),
+            pltpu.VMEM(table.shape, jnp.float32),
             pltpu.VMEM((tok, feat // 2), bf16),
             pltpu.VMEM((tok, feat // 2), bf16),
             pltpu.VMEM((layers, chips, tok, feat), bf16),
@@ -359,7 +369,7 @@
             pltpu.VMEM((layers, 2, 2, GRID_W, ROW_SPAN * GRID_W), jnp.float32),
             dma((layers, 3)),
             dma((layers,)),
-            dma((2,)),
+            dma((4,)),
             dma((3 + 4 * layers,)),
             dma((3 + 4 * layers,)),
             dma((layers, chips)),
@@ -370,7 +380,7 @@
             dma((layers, 5)),
         ],
         compiler_params=pltpu.CompilerParams(
-            collective_id=0, has_side_effects=True, vmem_limit_bytes=48 * 1024 * 1024
+            collective_id=0, has_side_effects=True, vmem_limit_bytes=67043328
         ),
         name="layers",
     )(hidden_in, norm_gain, query_weight, key_weight, value_weight, output_weight, table)

time: 146 us -> 141 us (0.966)
  local copies, waits for them, and re-layouts: 6.77 us -> 1.47 us
    unnamed x14 -> x1, local copies, waits for them, and re-layouts: 6.77 us -> 1.47 us
where the time goes in v2:
time: 141 us
  Pallas kernels  139 us (99%)
  local copies, waits for them, and re-layouts  1.47 us (1%)
    pallas_call x1, Pallas kernels, body(): pl.pallas_call(functools.partial(kernel, n_sp, n_tp, layers), out_shape=j...  139 us

profile of v2, /device:TPU:65, one launch (start us, length us, event | category | flops | bytes accessed | tf_op | source)
XLA Modules:
  0.0 140.7 jit_solution(11016696297650168422)
XLA Ops:
  0.0 139.2 %layers.1 = bf16[256,128]{1,0:T(8,128)(2,1)} custom-call(bf16[256,128]{1,0:T(8,128)(2,1)} %hid_ref.1, f32[3,2048]{1,0:T(4,128)} %gain_hbm.1, bf16[3,64,2048]{2,1,0:T(8,128)(2,1)} %wq_ref.1, bf16[3,64,2048]{2,1,0:T(8,128)(2,1)} %wk_ref.1, bf16[3,64,2048]{2,1,0:T(8,128)(2,1)} %wv_ref.1, bf16[3,1024,128]{2,1,0:T(8,128)(2,1)} %wo_ref.1, f32[3,15,1,31]{3,2,1,0:T(1,128)} %bitcast.1), custom_call_target="tpu_custom_call" | custom-call | tf_op jit(solution)/shard_map/layers/pallas_call | solution.py:352
  139.2 1.5 %copy.9 = bf16[256,128]{1,0:T(8,128)(2,1)} copy(bf16[256,128]{1,0:T(8,128)(2,1)} %layers.1) | data formatting | bytes 131072

commit v3 on v2

--- a/solution.py
+++ b/solution.py
@@ -47,6 +47,8 @@
     own_x_sem,
     d2d_s,
     d2d_r,
+    f_s,
+    f_r,
     x_s,
     x_r,
     a_s,
@@ -72,8 +74,7 @@
     def rows_at(start, size, align):
         return pl.ds(pl.multiple_of(start, align), size)
 
-    greet = [peer(j) for j in range(1, chips)]
-    greet += [{"tp": mate}]
+    greet = [{"tp": lax.rem(tp + j, n_tp)} for j in range(1, n_tp)]
     greet += [{"sp": z, "tp": t} for z in (up, down) for t in (tp, mate)]
     barrier = pltpu.get_barrier_semaphore()
     for device in greet:
@@ -81,9 +82,7 @@
 
     my_lanes = rows_at(core * half, half, half)
     own_x = [
-        pltpu.make_async_copy(
-            hid_ref.at[rows_at((1 - core) * tok, tok, tok), :], xst, own_x_sem.at[0]
-        ),
+        pltpu.make_async_copy(hid_ref, xst, own_x_sem.at[0]),
         pltpu.make_async_copy(
             hid_ref.at[rows_at(core * tok, tok, tok), :], xs.at[0, 0, :, my_lanes], own_x_sem.at[1]
         ),
@@ -142,7 +141,21 @@
         return copy
 
     own_x[0].wait()
-    x_mate = send(xst, xs.at[0, 0, :, my_lanes], d2d_s.at[0], d2d_r.at[0], {"tp": mate})
+    first_gather = [{}, {}]
+    for i in range(2):
+        spot = pl.ds(GRID_W * i, GRID_W)
+        given = xst.at[rows_at((1 - core) * tok + GRID_W * i, GRID_W, GRID_W), :]
+        kept = xst.at[rows_at(core * tok + GRID_W * i, GRID_W, GRID_W), :]
+        for j in ORDER + (0,):
+            far = (2 * j + 1 - 2 * core + n_tp) if j else (1 - 2 * core + n_tp)
+            there = xs.at[0, j, spot, my_lanes]
+            pair = []
+            if j:
+                pair.append(send(kept, there, f_s.at[i, 0, j], f_r.at[i, 0, j], peer(j)))
+            device = {"tp": lax.rem(tp + far, n_tp)}
+            pair.append(send(given, there, f_s.at[i, 1, j], f_r.at[i, 1, j], device))
+            first_gather[i][j] = pair
+    t_mate = send(tab.at[0], tab.at[2], d2d_s.at[1], d2d_r.at[1], {"tp": mate})
     w_mate = []
     sem = 2
     for layer in range(layers):
@@ -157,13 +170,6 @@
                 )
             )
             sem += 1
-        if layer == 0:
-            own_x[1].wait()
-            x_mate.wait_recv()
-            x_gather = [None] * chips
-            for j in ORDER:
-                x_gather[j] = send(xs.at[0, 0], xs.at[0, j], x_s.at[0, j], x_r.at[0, j], peer(j))
-            t_mate = send(tab.at[0], tab.at[2], d2d_s.at[1], d2d_r.at[1], {"tp": mate})
     o_mate = []
     for layer in range(layers):
         o_mate.append(
@@ -235,47 +241,118 @@
     make_bias()
     scale_layer(1)
 
-    my_rows = rows_at(256 + core * tok, tok, tok)
     lane_low = lax.broadcasted_iota(jnp.int32, (GRID_W, 128), 1) < HEAD_DIM
-
-    for layer in range(layers):
-        made = None
-        squares = None
-        for j in (0,) + ARRIVE:
-            if j:
-                x_gather[j].wait_recv()
-            block = xs[layer, j]
-            wide = block.astype(jnp.float32)
-            square = wide * wide
-            part = lax.dot_general(
-                block, wg[layer, j], (((1,), (1,)), ((), ())), preferred_element_type=jnp.float32
+    not_last = sp < n_sp - 1
+    not_first = sp > 0
+    places = [rows_at(256 + core * tok + GRID_W * i, GRID_W, GRID_W) for i in range(2)]
+
+    def halo_copies(layer, i):
+        mine = kv.at[layer, places[i], :]
+        above = kv.at[layer, rows_at(core * tok + GRID_W * i, GRID_W, GRID_W), :]
+        below = kv.at[layer, rows_at(512 + core * tok + GRID_W * i, GRID_W, GRID_W), :]
+        to_first = sp == 1
+        to_last = sp == n_sp - 2
+        at_first = sp == 0
+        at_last = sp == n_sp - 1
+        low = core == 0
+        high = core == 1
+        if i == 0:
+            down_same, down_same_got = not_first, not_last
+        else:
+            down_same, down_same_got = to_first, at_first
+        plan = (
+            (above, up, tp, not_last, not_first),
+            (below, down, tp, down_same, down_same_got),
+            (
+                above,
+                up,
+                mate,
+                not_last & (high | to_last),
+                not_first & (low | at_last),
+            ),
+            (
+                below,
+                down,
+                mate,
+                not_first & (low | to_first),
+                not_last & (high | at_first),
+            ),
+        )
+        copies = []
+        for n, (spot, z, t, sent, got) in enumerate(plan):
+            copy = pltpu.make_async_remote_copy(
+                src_ref=mine,
+                dst_ref=spot,
+                send_sem=h_s.at[layer, i, n + 1],
+                recv_sem=h_r.at[layer, i, n + 1],
+                device_id={"sp": z, "tp": t},
+                device_id_type=MESH,
             )
-            made = part if made is None else made + part
-            squares = square if squares is None else squares + square
-        mean = jnp.sum(squares, axis=1, keepdims=True) * (1.0 / (feat * chips))
-        normed = made * lax.rsqrt(mean + EPS)
-        queries = normed[:, 0:128].astype(jnp.bfloat16)
-        kv[layer, my_rows, :] = normed[:, 128:384].astype(jnp.bfloat16)
-        mine = kv.at[layer, my_rows, :]
-        halo = [send(mine, mine, h_s.at[layer, 0], h_r.at[layer, 0], {"tp": mate})]
-        above = kv.at[layer, rows_at(core * tok, tok, tok), :]
-        below = kv.at[layer, rows_at(512 + core * tok, tok, tok), :]
-        spots = ((above, up, tp), (below, down, tp), (above, up, mate), (below, down, mate))
-        for i, (spot, z, t) in enumerate(spots):
-            halo.append(
-                send(mine, spot, h_s.at[layer, i + 1], h_r.at[layer, i + 1], {"sp": z, "tp": t})
-            )
+            copies.append((copy, sent, got))
+        return mine, copies
+
+    conditional = []
+    x_gather = [[None] * chips for _ in range(2)]
+    for layer in range(layers):
+        queries = []
+        mates = []
+        halos = []
+        for i in range(2):
+            spot = slice(GRID_W * i, GRID_W * (i + 1))
+            if layer == 0:
+                order = [(j, first_gather[i][j]) for j in (0,) + ARRIVE]
+            else:
+                order = [(0, ())] + [(j, (x_gather[i][j],)) for j in ARRIVE]
+            made = None
+            squares = None
+            for j, copies in order:
+                if layer == 0 and i == 0 and j == 0:
+                    own_x[1].wait()
+                for copy in copies:
+                    copy.wait_recv()
+                block = xs[layer, j, spot]
+                wide = block.astype(jnp.float32)
+                square = wide * wide
+                part = lax.dot_general(
+                    block,
+                    wg[layer, j],
+                    (((1,), (1,)), ((), ())),
+                    preferred_element_type=jnp.float32,
+                )
+                made = part if made is None else made + part
+                squares = square if squares is None else squares + square
+            mean = jnp.sum(squares, axis=1, keepdims=True) * (1.0 / (feat * chips))
+            normed = made * lax.rsqrt(mean + EPS)
+            queries.append(normed[:, 0:128].astype(jnp.bfloat16))
+            kv[layer, places[i], :] = normed[:, 128:384].astype(jnp.bfloat16)
+            mine, copies = halo_copies(layer, i)
+            mates.append(send(mine, mine, h_s.at[layer, i, 0], h_r.at[layer, i, 0], {"tp": mate}))
+            for copy, sent, _ in copies:
+
+                @pl.when(sent)
+                def _(copy=copy):
+                    copy.start()
+
+            halos += copies
+            conditional += copies
         if layer == 0:
             for other in range(2, layers):
                 scale_layer(other)
-        for copy in halo:
+        for copy in mates:
             copy.wait_recv()
-
+        for copy, _, got in halos:
+
+            @pl.when(got)
+            def _(copy=copy):
+                copy.wait_recv()
+
+        gather = [[None] * chips for _ in range(2)]
         for i in range(2):
+            spot = pl.ds(GRID_W * i, GRID_W)
             outs = []
             for head in range(2):
                 pick = lane_low if head == 1 else jnp.logical_not(lane_low)
-                query = jnp.where(pick, queries[GRID_W * i : GRID_W * (i + 1)], 0)
+                query = jnp.where(pick, queries[i], 0)
                 pairs = kv[
                     layer,
                     rows_at(starts[i] * GRID_W, ROW_SPAN * GRID_W, GRID_W),
@@ -293,44 +370,65 @@
                 )
                 outs.append(mixed / total)
             both = jnp.where(lane_low, outs[0], outs[1])
-            atts[layer, 0, GRID_W * i : GRID_W * (i + 1), :] = both.astype(jnp.bfloat16)
-
-        gather = [None] * chips
-        for j in ORDER:
-            gather[j] = send(
-                atts.at[layer, 0], atts.at[layer, j], a_s.at[layer, j], a_r.at[layer, j], peer(j)
-            )
+            atts[layer, 0, spot, :] = both.astype(jnp.bfloat16)
+            for j in ORDER:
+                gather[i][j] = send(
+                    atts.at[layer, 0, spot, :],
+                    atts.at[layer, j, spot, :],
+                    a_s.at[layer, i, j],
+                    a_r.at[layer, i, j],
+                    peer(j),
+                )
+
         own_o[layer].wait()
         o_mate[layer].wait_recv()
-        stream = xs[layer, 0].astype(jnp.float32)
-        for j in (0,) + ARRIVE:
-            if j:
-                gather[j].wait_recv()
-            source = lax.rem(chip - j + chips, chips)
-            stream = stream + jnp.dot(
-                atts[layer, j],
-                wout[layer, rows_at(source * 128, 128, 128), :],
-                preferred_element_type=jnp.float32,
-            )
-        if layer + 1 < layers:
-            xs[layer + 1, 0] = stream.astype(jnp.bfloat16)
-            for j in ORDER:
-                x_gather[j] = send(
-                    xs.at[layer + 1, 0],
-                    xs.at[layer + 1, j],
-                    x_s.at[layer + 1, j],
-                    x_r.at[layer + 1, j],
-                    peer(j),
-                )
-        else:
+        last = []
+        for i in range(2):
+            spot = pl.ds(GRID_W * i, GRID_W)
+            stream = xs[layer, 0, spot].astype(jnp.float32)
+            for j in (0,) + ARRIVE:
+                if j:
+                    gather[i][j].wait_recv()
+                source = lax.rem(chip - j + chips, chips)
+                stream = stream + jnp.dot(
+                    atts[layer, j, spot],
+                    wout[layer, rows_at(source * 128, 128, 128), :],
+                    preferred_element_type=jnp.float32,
+                )
             final = stream.astype(jnp.bfloat16)
-            swap = core == 0
-            keep = jnp.where(swap, final[:, 0:half], final[:, half:feat])
-            last_half[...] = jnp.where(swap, final[:, half:feat], final[:, 0:half])
-            place = rows_at(core * tok, tok, tok)
-            last = send(last_half, out_ref.at[place, :], d2d_s.at[sem], d2d_r.at[sem], {"tp": mate})
-            out_ref[place, :] = keep
-            last.wait_recv()
+            if layer + 1 < layers:
+                xs[layer + 1, 0, spot, :] = final
+                for j in ORDER:
+                    x_gather[i][j] = send(
+                        xs.at[layer + 1, 0, spot, :],
+                        xs.at[layer + 1, j, spot, :],
+                        x_s.at[layer, i, j],
+                        x_r.at[layer, i, j],
+                        peer(j),
+                    )
+            else:
+                swap = core == 0
+                last_half[spot, :] = jnp.where(swap, final[:, half:feat], final[:, 0:half])
+                place = rows_at(core * tok + GRID_W * i, GRID_W, GRID_W)
+                last.append(
+                    send(
+                        last_half.at[spot, :],
+                        out_ref.at[place, :],
+                        d2d_s.at[sem],
+                        d2d_r.at[sem],
+                        {"tp": mate},
+                    )
+                )
+                sem += 1
+                out_ref[place, :] = jnp.where(swap, final[:, 0:half], final[:, half:feat])
+        for copy in last:
+            copy.wait_recv()
+    for copy, sent, _ in conditional:
+
+        @pl.when(sent)
+        def _(copy=copy):
+            copy.wait_send()
+
     for copy in sends:
         copy.wait_send()
 
@@ -357,7 +455,7 @@
         scratch_shapes=[
             pltpu.VMEM(norm_gain.shape, jnp.float32),
             pltpu.VMEM(table.shape, jnp.float32),
-            pltpu.VMEM((tok, feat // 2), bf16),
+            pltpu.VMEM((tokens, feat // 2), bf16),
             pltpu.VMEM((tok, feat // 2), bf16),
             pltpu.VMEM((layers, chips, tok, feat), bf16),
             pltpu.VMEM((layers, chips, tok, 128), bf16),
@@ -370,14 +468,16 @@
             dma((layers, 3)),
             dma((layers,)),
             dma((4,)),
-            dma((3 + 4 * layers,)),
-            dma((3 + 4 * layers,)),
-            dma((layers, chips)),
-            dma((layers, chips)),
-            dma((layers, chips)),
-            dma((layers, chips)),
-            dma((layers, 5)),
-            dma((layers, 5)),
+            dma((4 + 4 * layers,)),
+            dma((4 + 4 * layers,)),
+            dma((2, 2, chips)),
+            dma((2, 2, chips)),
+            dma((layers, 2, chips)),
+            dma((layers, 2, chips)),
+            dma((layers, 2, chips)),
+            dma((layers, 2, chips)),
+            dma((layers, 2, 5)),
+            dma((layers, 2, 5)),
         ],
         compiler_params=pltpu.CompilerParams(
             collective_id=0, has_side_effects=True, vmem_limit_bytes=67043328

time: 141 us -> 126 us (0.89)
  Pallas kernels: 139 us -> 124 us
    pallas_call x1, Pallas kernels: 139 us -> 124 us  [body(): pl.pallas_call(functools.partial(kernel, n_sp, n_tp, layers), out_shape=j...]
where the time goes in v3:
time: 126 us; the launch traced here: 125 us
  Pallas kernels  124 us (98%)
  local copies, waits for them, and re-layouts  1.47 us (1%)
    pallas_call x1, Pallas kernels, body(): pl.pallas_call(functools.partial(kernel, n_sp, n_tp, layers), out_shape=j...  124 us

profile of v3, /device:TPU:65, one launch (start us, length us, event | category | flops | bytes accessed | tf_op | source)
XLA Modules:
  0.0 125.4 jit_solution(8013619741585787056)
XLA Ops:
  0.0 123.9 %layers.1 = bf16[256,128]{1,0:T(8,128)(2,1)} custom-call(bf16[256,128]{1,0:T(8,128)(2,1)} %hid_ref.1, f32[3,2048]{1,0:T(4,128)} %gain_hbm.1, bf16[3,64,2048]{2,1,0:T(8,128)(2,1)} %wq_ref.1, bf16[3,64,2048]{2,1,0:T(8,128)(2,1)} %wk_ref.1, bf16[3,64,2048]{2,1,0:T(8,128)(2,1)} %wv_ref.1, bf16[3,1024,128]{2,1,0:T(8,128)(2,1)} %wo_ref.1, f32[3,15,1,31]{3,2,1,0:T(1,128)} %bitcast.1), custom_call_target="tpu_custom_call" | custom-call | tf_op jit(solution)/shard_map/layers/pallas_call | solution.py:450
  123.9 1.5 %copy.9 = bf16[256,128]{1,0:T(8,128)(2,1)} copy(bf16[256,128]{1,0:T(8,128)(2,1)} %layers.1) | data formatting | bytes 131072

commit v4 on v3

--- a/solution.py
+++ b/solution.py
@@ -16,6 +16,8 @@
 MESH = pl.DeviceIdType.MESH
 ORDER = (4, 3, 5, 2, 6, 1, 7)
 ARRIVE = (1, 7, 2, 6, 3, 5, 4)
+HELD = (0, 5, 3)
+HANDED = ((0, 1, 1), (0, -1, 7), (5, 1, 6), (5, -1, 4), (3, -1, 2))
 
 
 def kernel(
@@ -49,6 +51,8 @@
     d2d_r,
     f_s,
     f_r,
+    e_s,
+    e_r,
     x_s,
     x_r,
     a_s,
@@ -69,7 +73,7 @@
     down = lax.rem(sp + n_sp - 1, n_sp)
 
     def peer(j):
-        return {"tp": lax.rem(tp + 2 * j, n_tp)}
+        return {"tp": lax.rem(tp + 2 * j + n_tp, n_tp)}
 
     def rows_at(start, size, align):
         return pl.ds(pl.multiple_of(start, align), size)
@@ -107,7 +111,7 @@
             own_w.append(copy)
     for layer in range(layers):
         copy = pltpu.make_async_copy(
-            wo_ref.at[layer], wout.at[layer, :, my_lanes], own_o_sem.at[layer]
+            wo_ref.at[layer], wout.at[layer, 0, :, my_lanes], own_o_sem.at[layer]
         )
         copy.start()
         own_o.append(copy)
@@ -175,7 +179,7 @@
         o_mate.append(
             send(
                 wo_ref.at[layer],
-                wout.at[layer, :, my_lanes],
+                wout.at[layer, 0, :, my_lanes],
                 d2d_s.at[sem],
                 d2d_r.at[sem],
                 {"tp": mate},
@@ -292,7 +296,7 @@
         return mine, copies
 
     conditional = []
-    x_gather = [[None] * chips for _ in range(2)]
+    x_gather = [[], []]
     for layer in range(layers):
         queries = []
         mates = []
@@ -302,7 +306,7 @@
             if layer == 0:
                 order = [(j, first_gather[i][j]) for j in (0,) + ARRIVE]
             else:
-                order = [(0, ())] + [(j, (x_gather[i][j],)) for j in ARRIVE]
+                order = [(j, ()) for j in HELD] + x_gather[i]
             made = None
             squares = None
             for j, copies in order:
@@ -321,6 +325,18 @@
                 )
                 made = part if made is None else made + part
                 squares = square if squares is None else squares + square
+            if i == 0 and layer + 1 < layers:
+                shipped = []
+                for n, away in ((1, -3), (2, 3)):
+                    shipped.append(
+                        send(
+                            wo_ref.at[layer],
+                            wout.at[layer, n, :, my_lanes],
+                            e_s.at[layer, 0, n - 1],
+                            e_r.at[layer, 0, n - 1],
+                            peer(away),
+                        )
+                    )
             mean = jnp.sum(squares, axis=1, keepdims=True) * (1.0 / (feat * chips))
             normed = made * lax.rsqrt(mean + EPS)
             queries.append(normed[:, 0:128].astype(jnp.bfloat16))
@@ -382,30 +398,54 @@
 
         own_o[layer].wait()
         o_mate[layer].wait_recv()
+        held = HELD[:1]
+        if layer + 1 < layers:
+            held = HELD
+            relayed = []
+            for n in (1, 2):
+                shipped[n - 1].wait_recv()
+                spot = wout.at[layer, n, :, my_lanes]
+                relayed.append(
+                    send(
+                        spot,
+                        spot,
+                        e_s.at[layer, 1, n - 1],
+                        e_r.at[layer, 1, n - 1],
+                        {"tp": mate},
+                    )
+                )
+            for copy in relayed:
+                copy.wait_recv()
         last = []
         for i in range(2):
             spot = pl.ds(GRID_W * i, GRID_W)
-            stream = xs[layer, 0, spot].astype(jnp.float32)
+            streams = [xs[layer, slot, spot].astype(jnp.float32) for slot in held]
             for j in (0,) + ARRIVE:
                 if j:
                     gather[i][j].wait_recv()
                 source = lax.rem(chip - j + chips, chips)
-                stream = stream + jnp.dot(
-                    atts[layer, j, spot],
-                    wout[layer, rows_at(source * 128, 128, 128), :],
-                    preferred_element_type=jnp.float32,
-                )
-            final = stream.astype(jnp.bfloat16)
+                block = atts[layer, j, spot]
+                for n in range(len(held)):
+                    streams[n] = streams[n] + jnp.dot(
+                        block,
+                        wout[layer, n, rows_at(source * 128, 128, 128), :],
+                        preferred_element_type=jnp.float32,
+                    )
+            finals = [stream.astype(jnp.bfloat16) for stream in streams]
+            final = finals[0]
             if layer + 1 < layers:
-                xs[layer + 1, 0, spot, :] = final
-                for j in ORDER:
-                    x_gather[i][j] = send(
-                        xs.at[layer + 1, 0, spot, :],
-                        xs.at[layer + 1, j, spot, :],
-                        x_s.at[layer, i, j],
-                        x_r.at[layer, i, j],
-                        peer(j),
+                for slot, block in zip(held, finals, strict=True):
+                    xs[layer + 1, slot, spot, :] = block
+                x_gather[i] = []
+                for slot, far, there in HANDED:
+                    copy = send(
+                        xs.at[layer + 1, slot, spot, :],
+                        xs.at[layer + 1, there, spot, :],
+                        x_s.at[layer, i, there],
+                        x_r.at[layer, i, there],
+                        peer(far),
                     )
+                    x_gather[i].append((there, (copy,)))
             else:
                 swap = core == 0
                 last_half[spot, :] = jnp.where(swap, final[:, half:feat], final[:, 0:half])
@@ -462,7 +502,7 @@
             pltpu.VMEM((layers, 768, 256), bf16),
             pltpu.VMEM((layers, 384, width), bf16),
             pltpu.VMEM((layers, chips, 384, feat), bf16),
-            pltpu.VMEM((layers, 1024, feat), bf16),
+            pltpu.VMEM((layers, 3, 1024, feat), bf16),
             pltpu.VMEM((3, layers, 16, 128), jnp.float32),
             pltpu.VMEM((layers, 2, 2, GRID_W, ROW_SPAN * GRID_W), jnp.float32),
             dma((layers, 3)),
@@ -472,6 +512,8 @@
             dma((4 + 4 * layers,)),
             dma((2, 2, chips)),
             dma((2, 2, chips)),
+            dma((layers, 2, 2)),
+            dma((layers, 2, 2)),
             dma((layers, 2, chips)),
             dma((layers, 2, chips)),
             dma((layers, 2, chips)),

time: 126 us -> 134 us (1.063)
  Pallas kernels: 124 us -> 132 us
    pallas_call x1, Pallas kernels: 124 us -> 132 us  [body(): pl.pallas_call(functools.partial(kernel, n_sp, n_tp, layers), out_shape=j...]
where the time goes in v4:
time: 134 us
  Pallas kernels  132 us (99%)
  local copies, waits for them, and re-layouts  1.47 us (1%)
    pallas_call x1, Pallas kernels, body(): pl.pallas_call(functools.partial(kernel, n_sp, n_tp, layers), out_shape=j...  132 us

profile of v4, /device:TPU:65, one launch (start us, length us, event | category | flops | bytes accessed | tf_op | source)
XLA Modules:
  0.0 133.9 jit_solution(15825020787292091289)
XLA Ops:
  0.0 132.4 %layers.1 = bf16[256,128]{1,0:T(8,128)(2,1)} custom-call(bf16[256,128]{1,0:T(8,128)(2,1)} %hid_ref.1, f32[3,2048]{1,0:T(4,128)} %gain_hbm.1, bf16[3,64,2048]{2,1,0:T(8,128)(2,1)} %wq_ref.1, bf16[3,64,2048]{2,1,0:T(8,128)(2,1)} %wk_ref.1, bf16[3,64,2048]{2,1,0:T(8,128)(2,1)} %wv_ref.1, bf16[3,1024,128]{2,1,0:T(8,128)(2,1)} %wo_ref.1, f32[3,15,1,31]{3,2,1,0:T(1,128)} %bitcast.1), custom_call_target="tpu_custom_call" | custom-call | tf_op jit(solution)/shard_map/layers/pallas_call | solution.py:490
  132.4 1.5 %copy.9 = bf16[256,128]{1,0:T(8,128)(2,1)} copy(bf16[256,128]{1,0:T(8,128)(2,1)} %layers.1) | data formatting | bytes 131072

commit v5 on v3

--- a/solution.py
+++ b/solution.py
@@ -14,8 +14,9 @@
 EPS = 1e-06
 NEG = -1e30
 MESH = pl.DeviceIdType.MESH
-ORDER = (4, 3, 5, 2, 6, 1, 7)
+ORDER = (2, 6, 1, 7)
 ARRIVE = (1, 7, 2, 6, 3, 5, 4)
+HAND = (((2, 2, 4), (2, 1, 3), (6, -1, 5)), ((6, -2, 4), (6, -1, 5), (2, 1, 3)))
 
 
 def kernel(
@@ -69,7 +70,7 @@
     down = lax.rem(sp + n_sp - 1, n_sp)
 
     def peer(j):
-        return {"tp": lax.rem(tp + 2 * j, n_tp)}
+        return {"tp": lax.rem(tp + 2 * j + n_tp, n_tp)}
 
     def rows_at(start, size, align):
         return pl.ds(pl.multiple_of(start, align), size)
@@ -291,25 +292,40 @@
             copies.append((copy, sent, got))
         return mine, copies
 
+    def arrive(coming, slot):
+        for copy in coming.pop(slot, ()):
+            copy.wait_recv()
+
+    def hand_on(array, spot, coming, s_sems, r_sems, i):
+        for came, far, there in HAND[i]:
+            arrive(coming, came)
+            coming[there] = [
+                send(
+                    array.at[came, spot, :],
+                    array.at[there, spot, :],
+                    s_sems.at[i, there],
+                    r_sems.at[i, there],
+                    peer(far),
+                )
+            ]
+
     conditional = []
-    x_gather = [[None] * chips for _ in range(2)]
+    x_gather = first_gather
     for layer in range(layers):
         queries = []
         mates = []
         halos = []
         for i in range(2):
+            spot = pl.ds(GRID_W * i, GRID_W)
+            hand_on(xs.at[layer], spot, x_gather[i], x_s.at[layer], x_r.at[layer], i)
+        for i in range(2):
             spot = slice(GRID_W * i, GRID_W * (i + 1))
-            if layer == 0:
-                order = [(j, first_gather[i][j]) for j in (0,) + ARRIVE]
-            else:
-                order = [(0, ())] + [(j, (x_gather[i][j],)) for j in ARRIVE]
             made = None
             squares = None
-            for j, copies in order:
+            for j in (0,) + ARRIVE:
                 if layer == 0 and i == 0 and j == 0:
                     own_x[1].wait()
-                for copy in copies:
-                    copy.wait_recv()
+                arrive(x_gather[i], j)
                 block = xs[layer, j, spot]
                 wide = block.astype(jnp.float32)
                 square = wide * wide
@@ -346,7 +362,8 @@
             def _(copy=copy):
                 copy.wait_recv()
 
-        gather = [[None] * chips for _ in range(2)]
+        gather = [{}, {}]
+        x_gather = [{}, {}]
         for i in range(2):
             spot = pl.ds(GRID_W * i, GRID_W)
             outs = []
@@ -372,13 +389,17 @@
             both = jnp.where(lane_low, outs[0], outs[1])
             atts[layer, 0, spot, :] = both.astype(jnp.bfloat16)
             for j in ORDER:
-                gather[i][j] = send(
+                copy = send(
                     atts.at[layer, 0, spot, :],
                     atts.at[layer, j, spot, :],
                     a_s.at[layer, i, j],
                     a_r.at[layer, i, j],
                     peer(j),
                 )
+                gather[i][j] = [copy]
+        for i in range(2):
+            spot = pl.ds(GRID_W * i, GRID_W)
+            hand_on(atts.at[layer], spot, gather[i], a_s.at[layer], a_r.at[layer], i)
 
         own_o[layer].wait()
         o_mate[layer].wait_recv()
@@ -387,8 +408,7 @@
             spot = pl.ds(GRID_W * i, GRID_W)
             stream = xs[layer, 0, spot].astype(jnp.float32)
             for j in (0,) + ARRIVE:
-                if j:
-                    gather[i][j].wait_recv()
+                arrive(gather[i], j)
                 source = lax.rem(chip - j + chips, chips)
                 stream = stream + jnp.dot(
                     atts[layer, j, spot],
@@ -399,13 +419,14 @@
             if layer + 1 < layers:
                 xs[layer + 1, 0, spot, :] = final
                 for j in ORDER:
-                    x_gather[i][j] = send(
+                    copy = send(
                         xs.at[layer + 1, 0, spot, :],
                         xs.at[layer + 1, j, spot, :],
-                        x_s.at[layer, i, j],
-                        x_r.at[layer, i, j],
+                        x_s.at[layer + 1, i, j],
+                        x_r.at[layer + 1, i, j],
                         peer(j),
                     )
+                    x_gather[i][j] = [copy]
             else:
                 swap = core == 0
                 last_half[spot, :] = jnp.where(swap, final[:, half:feat], final[:, 0:half])

time: 126 us -> 118 us (0.937)
  Pallas kernels: 124 us -> 116 us
    pallas_call x1, Pallas kernels: 124 us -> 116 us  [body(): pl.pallas_call(functools.partial(kernel, n_sp, n_tp, layers), out_shape=j...]
where the time goes in v5:
time: 118 us
  Pallas kernels  116 us (98%)
  local copies, waits for them, and re-layouts  1.47 us (1%)
    pallas_call x1, Pallas kernels, body(): pl.pallas_call(functools.partial(kernel, n_sp, n_tp, layers), out_shape=j...  116 us

profile of v5, /device:TPU:65, one launch (start us, length us, event | category | flops | bytes accessed | tf_op | source)
XLA Modules:
  0.0 117.7 jit_solution(7298387931477283913)
XLA Ops:
  0.0 116.3 %layers.1 = bf16[256,128]{1,0:T(8,128)(2,1)} custom-call(bf16[256,128]{1,0:T(8,128)(2,1)} %hid_ref.1, f32[3,2048]{1,0:T(4,128)} %gain_hbm.1, bf16[3,64,2048]{2,1,0:T(8,128)(2,1)} %wq_ref.1, bf16[3,64,2048]{2,1,0:T(8,128)(2,1)} %wk_ref.1, bf16[3,64,2048]{2,1,0:T(8,128)(2,1)} %wv_ref.1, bf16[3,1024,128]{2,1,0:T(8,128)(2,1)} %wo_ref.1, f32[3,15,1,31]{3,2,1,0:T(1,128)} %bitcast.1), custom_call_target="tpu_custom_call" | custom-call | tf_op jit(solution)/shard_map/layers/pallas_call | solution.py:471
  116.3 1.5 %copy.9 = bf16[256,128]{1,0:T(8,128)(2,1)} copy(bf16[256,128]{1,0:T(8,128)(2,1)} %layers.1) | data formatting | bytes 131072

commit v6 on v5

--- a/solution.py
+++ b/solution.py
@@ -16,7 +16,13 @@
 MESH = pl.DeviceIdType.MESH
 ORDER = (2, 6, 1, 7)
 ARRIVE = (1, 7, 2, 6, 3, 5, 4)
-HAND = (((2, 2, 4), (2, 1, 3), (6, -1, 5)), ((6, -2, 4), (6, -1, 5), (2, 1, 3)))
+HALF = GRID_W // 2
+HAND = (
+    (2, 2, 4, (0, HALF), 4),
+    (2, 1, 3, (0, GRID_W), 3),
+    (6, -2, 4, (HALF, HALF), 0),
+    (6, -1, 5, (0, GRID_W), 5),
+)
 
 
 def kernel(
@@ -75,7 +81,8 @@
     def rows_at(start, size, align):
         return pl.ds(pl.multiple_of(start, align), size)
 
-    greet = [{"tp": lax.rem(tp + j, n_tp)} for j in range(1, n_tp)]
+    greet = [peer(j) for j in ORDER] + [{"tp": mate}]
+    greet += [{"tp": lax.rem(mate + 2 * j, n_tp)} for j in ORDER]
     greet += [{"sp": z, "tp": t} for z in (up, down) for t in (tp, mate)]
     barrier = pltpu.get_barrier_semaphore()
     for device in greet:
@@ -296,18 +303,18 @@
         for copy in coming.pop(slot, ()):
             copy.wait_recv()
 
-    def hand_on(array, spot, coming, s_sems, r_sems, i):
-        for came, far, there in HAND[i]:
+    def hand_on(array, row, coming, s_sems, r_sems):
+        for came, far, there, (first, size), sem in HAND:
             arrive(coming, came)
-            coming[there] = [
-                send(
-                    array.at[came, spot, :],
-                    array.at[there, spot, :],
-                    s_sems.at[i, there],
-                    r_sems.at[i, there],
-                    peer(far),
-                )
-            ]
+            spot = pl.ds(GRID_W * row + first, size)
+            copy = send(
+                array.at[came, spot, :],
+                array.at[there, spot, :],
+                s_sems.at[row, sem],
+                r_sems.at[row, sem],
+                peer(far),
+            )
+            coming.setdefault(there, []).append(copy)
 
     conditional = []
     x_gather = first_gather
@@ -316,8 +323,7 @@
         mates = []
         halos = []
         for i in range(2):
-            spot = pl.ds(GRID_W * i, GRID_W)
-            hand_on(xs.at[layer], spot, x_gather[i], x_s.at[layer], x_r.at[layer], i)
+            hand_on(xs.at[layer], i, x_gather[i], x_s.at[layer], x_r.at[layer])
         for i in range(2):
             spot = slice(GRID_W * i, GRID_W * (i + 1))
             made = None
@@ -397,9 +403,12 @@
                     peer(j),
                 )
                 gather[i][j] = [copy]
+        before = list(sends[: -2 * len(ORDER)])
+        del sends[: len(before)]
         for i in range(2):
-            spot = pl.ds(GRID_W * i, GRID_W)
-            hand_on(atts.at[layer], spot, gather[i], a_s.at[layer], a_r.at[layer], i)
+            hand_on(atts.at[layer], i, gather[i], a_s.at[layer], a_r.at[layer])
+        for copy in before:
+            copy.wait_send()
 
         own_o[layer].wait()
         o_mate[layer].wait_recv()

time: 118 us -> 118 us (level)
  no operation moved by 1% of the time
where the time goes in v6:
time: 118 us
  Pallas kernels  116 us (98%)
  local copies, waits for them, and re-layouts  1.47 us (1%)
    pallas_call x1, Pallas kernels, body(): pl.pallas_call(functools.partial(kernel, n_sp, n_tp, layers), out_shape=j...  116 us

profile of v6, /device:TPU:65, one launch (start us, length us, event | category | flops | bytes accessed | tf_op | source)
XLA Modules:
  0.0 117.9 jit_solution(6380030256538146885)
XLA Ops:
  0.0 116.4 %layers.1 = bf16[256,128]{1,0:T(8,128)(2,1)} custom-call(bf16[256,128]{1,0:T(8,128)(2,1)} %hid_ref.1, f32[3,2048]{1,0:T(4,128)} %gain_hbm.1, bf16[3,64,2048]{2,1,0:T(8,128)(2,1)} %wq_ref.1, bf16[3,64,2048]{2,1,0:T(8,128)(2,1)} %wk_ref.1, bf16[3,64,2048]{2,1,0:T(8,128)(2,1)} %wv_ref.1, bf16[3,1024,128]{2,1,0:T(8,128)(2,1)} %wo_ref.1, f32[3,15,1,31]{3,2,1,0:T(1,128)} %bitcast.1), custom_call_target="tpu_custom_call" | custom-call | tf_op jit(solution)/shard_map/layers/pallas_call | solution.py:480
  116.4 1.5 %copy.9 = bf16[256,128]{1,0:T(8,128)(2,1)} copy(bf16[256,128]{1,0:T(8,128)(2,1)} %layers.1) | data formatting | bytes 131072

commit v7 on v6

--- a/solution.py
+++ b/solution.py
@@ -41,6 +41,7 @@
     ob_ref,
     xst,
     last_half,
+    kept_half,
     xs,
     atts,
     kv,
@@ -244,10 +245,6 @@
 
         lax.fori_loop(0, layers, one, 0)
 
-    own_g.wait()
-    scale_layer(0)
-    make_bias()
-    scale_layer(1)
 
     lane_low = lax.broadcasted_iota(jnp.int32, (GRID_W, 128), 1) < HEAD_DIM
     not_last = sp < n_sp - 1
@@ -324,13 +321,17 @@
         halos = []
         for i in range(2):
             hand_on(xs.at[layer], i, x_gather[i], x_s.at[layer], x_r.at[layer])
+        if layer == 0:
+            own_g.wait()
+            own_x[1].wait()
+            scale_layer(0)
+            make_bias()
+            scale_layer(1)
         for i in range(2):
             spot = slice(GRID_W * i, GRID_W * (i + 1))
             made = None
             squares = None
             for j in (0,) + ARRIVE:
-                if layer == 0 and i == 0 and j == 0:
-                    own_x[1].wait()
                 arrive(x_gather[i], j)
                 block = xs[layer, j, spot]
                 wide = block.astype(jnp.float32)
@@ -413,6 +414,7 @@
         own_o[layer].wait()
         o_mate[layer].wait_recv()
         last = []
+        kept = []
         for i in range(2):
             spot = pl.ds(GRID_W * i, GRID_W)
             stream = xs[layer, 0, spot].astype(jnp.float32)
@@ -450,9 +452,16 @@
                     )
                 )
                 sem += 1
-                out_ref[place, :] = jnp.where(swap, final[:, 0:half], final[:, half:feat])
+                kept_half[spot, :] = jnp.where(swap, final[:, 0:half], final[:, half:feat])
+                copy = pltpu.make_async_copy(
+                    kept_half.at[spot, :], out_ref.at[place, :], own_x_sem.at[4 + i]
+                )
+                copy.start()
+                kept.append(copy)
         for copy in last:
             copy.wait_recv()
+        for copy in kept:
+            copy.wait()
     for copy, sent, _ in conditional:
 
         @pl.when(sent)
@@ -473,7 +482,6 @@
     tok = tokens // 2
     feat = width // chips
     any_space = pl.BlockSpec(memory_space=pltpu.HBM)
-    vmem = pl.BlockSpec(memory_space=pltpu.VMEM)
     dma = pltpu.SemaphoreType.DMA
     bf16 = jnp.bfloat16
     table = offset_bias.transpose(0, 2, 1, 3)
@@ -481,11 +489,12 @@
         functools.partial(kernel, n_sp, n_tp, layers),
         out_shape=jax.ShapeDtypeStruct(hidden_in.shape, bf16),
         in_specs=[any_space] * 7,
-        out_specs=vmem,
+        out_specs=any_space,
         scratch_shapes=[
             pltpu.VMEM(norm_gain.shape, jnp.float32),
             pltpu.VMEM(table.shape, jnp.float32),
             pltpu.VMEM((tokens, feat // 2), bf16),
+            pltpu.VMEM((tok, feat // 2), bf16),
             pltpu.VMEM((tok, feat // 2), bf16),
             pltpu.VMEM((layers, chips, tok, feat), bf16),
             pltpu.VMEM((layers, chips, tok, 128), bf16),
@@ -497,7 +506,7 @@
             pltpu.VMEM((layers, 2, 2, GRID_W, ROW_SPAN * GRID_W), jnp.float32),
             dma((layers, 3)),
             dma((layers,)),
-            dma((4,)),
+            dma((6,)),
             dma((4 + 4 * layers,)),
             dma((4 + 4 * layers,)),
             dma((2, 2, chips)),

time: 118 us -> 117 us (level)
  no operation moved by 1% of the time
where the time goes in v7:
time: 117 us
  Pallas kernels  115 us (98%)
  local copies, waits for them, and re-layouts  1.47 us (1%)
    pallas_call x1, Pallas kernels, body(): pl.pallas_call(functools.partial(kernel, n_sp, n_tp, layers), out_shape=j...  115 us

profile of v7, /device:TPU:65, one launch (start us, length us, event | category | flops | bytes accessed | tf_op | source)
XLA Modules:
  0.0 116.9 jit_solution(1032965817497083835)
XLA Ops:
  0.0 115.5 %layers.1 = bf16[256,128]{1,0:T(8,128)(2,1)} custom-call(bf16[256,128]{1,0:T(8,128)(2,1)} %hid_ref.1, f32[3,2048]{1,0:T(4,128)} %gain_hbm.1, bf16[3,64,2048]{2,1,0:T(8,128)(2,1)} %wq_ref.1, bf16[3,64,2048]{2,1,0:T(8,128)(2,1)} %wk_ref.1, bf16[3,64,2048]{2,1,0:T(8,128)(2,1)} %wv_ref.1, bf16[3,1024,128]{2,1,0:T(8,128)(2,1)} %wo_ref.1, f32[3,15,1,31]{3,2,1,0:T(1,128)} %bitcast.1), custom_call_target="tpu_custom_call" | custom-call | tf_op jit(solution)/shard_map/layers/pallas_call | solution.py:488
  115.5 1.5 %copy.9 = bf16[256,128]{1,0:T(8,128)(2,1)} copy(bf16[256,128]{1,0:T(8,128)(2,1)} %layers.1) | data formatting | bytes 131072

commit v8 on v7

--- a/solution.py
+++ b/solution.py
@@ -166,31 +166,20 @@
             first_gather[i][j] = pair
     t_mate = send(tab.at[0], tab.at[2], d2d_s.at[1], d2d_r.at[1], {"tp": mate})
     w_mate = []
-    sem = 2
-    for layer in range(layers):
-        for i, w_ref in enumerate((wq_ref, wk_ref, wv_ref)):
-            w_mate.append(
-                send(
-                    w_ref.at[layer],
-                    wraw.at[layer, w_rows[i], :],
-                    d2d_s.at[sem],
-                    d2d_r.at[sem],
-                    {"tp": mate},
-                )
-            )
-            sem += 1
     o_mate = []
-    for layer in range(layers):
-        o_mate.append(
-            send(
-                wo_ref.at[layer],
-                wout.at[layer, :, my_lanes],
-                d2d_s.at[sem],
-                d2d_r.at[sem],
-                {"tp": mate},
-            )
-        )
-        sem += 1
+
+    def give_weights(layer):
+        sem = 2 + 4 * layer
+        pairs = [
+            (w_ref.at[layer], wraw.at[layer, rows, :])
+            for w_ref, rows in zip((wq_ref, wk_ref, wv_ref), w_rows, strict=True)
+        ]
+        pairs.append((wo_ref.at[layer], wout.at[layer, :, my_lanes]))
+        for i, (mine, there) in enumerate(pairs):
+            copy = send(mine, there, d2d_s.at[sem + i], d2d_r.at[sem + i], {"tp": mate})
+            (w_mate if i < 3 else o_mate).append(copy)
+
+    give_weights(0)
 
     def scale_layer(layer):
         for copy in own_w[3 * layer : 3 * layer + 3]:
@@ -324,9 +313,8 @@
         if layer == 0:
             own_g.wait()
             own_x[1].wait()
-            scale_layer(0)
             make_bias()
-            scale_layer(1)
+        scale_layer(layer)
         for i in range(2):
             spot = slice(GRID_W * i, GRID_W * (i + 1))
             made = None
@@ -358,9 +346,6 @@
 
             halos += copies
             conditional += copies
-        if layer == 0:
-            for other in range(2, layers):
-                scale_layer(other)
         for copy in mates:
             copy.wait_recv()
         for copy, _, got in halos:
@@ -408,6 +393,8 @@
         del sends[: len(before)]
         for i in range(2):
             hand_on(atts.at[layer], i, gather[i], a_s.at[layer], a_r.at[layer])
+        if layer + 1 < layers:
+            give_weights(layer + 1)
         for copy in before:
             copy.wait_send()
 
@@ -446,12 +433,11 @@
                     send(
                         last_half.at[spot, :],
                         out_ref.at[place, :],
-                        d2d_s.at[sem],
-                        d2d_r.at[sem],
+                        d2d_s.at[2 + 4 * layers + i],
+                        d2d_r.at[2 + 4 * layers + i],
                         {"tp": mate},
                     )
                 )
-                sem += 1
                 kept_half[spot, :] = jnp.where(swap, final[:, 0:half], final[:, half:feat])
                 copy = pltpu.make_async_copy(
                     kept_half.at[spot, :], out_ref.at[place, :], own_x_sem.at[4 + i]

time: 117 us -> 117 us (level)
  no operation moved by 1% of the time
where the time goes in v8:
time: 117 us
  Pallas kernels  116 us (99%)
  local copies, waits for them, and re-layouts  1.47 us (1%)
    pallas_call x1, Pallas kernels, body(): pl.pallas_call(functools.partial(kernel, n_sp, n_tp, layers), out_shape=j...  116 us

profile of v8, /device:TPU:65, one launch (start us, length us, event | category | flops | bytes accessed | tf_op | source)
XLA Modules:
  0.0 117.3 jit_solution(15411146570245034659)
XLA Ops:
  0.0 115.8 %layers.1 = bf16[256,128]{1,0:T(8,128)(2,1)} custom-call(bf16[256,128]{1,0:T(8,128)(2,1)} %hid_ref.1, f32[3,2048]{1,0:T(4,128)} %gain_hbm.1, bf16[3,64,2048]{2,1,0:T(8,128)(2,1)} %wq_ref.1, bf16[3,64,2048]{2,1,0:T(8,128)(2,1)} %wk_ref.1, bf16[3,64,2048]{2,1,0:T(8,128)(2,1)} %wv_ref.1, bf16[3,1024,128]{2,1,0:T(8,128)(2,1)} %wo_ref.1, f32[3,15,1,31]{3,2,1,0:T(1,128)} %bitcast.1), custom_call_target="tpu_custom_call" | custom-call | tf_op jit(solution)/shard_map/layers/pallas_call | solution.py:474
  115.8 1.5 %copy.9 = bf16[256,128]{1,0:T(8,128)(2,1)} copy(bf16[256,128]{1,0:T(8,128)(2,1)} %layers.1) | data formatting | bytes 131072

commit v9 on v8

--- a/solution.py
+++ b/solution.py
@@ -14,15 +14,9 @@
 EPS = 1e-06
 NEG = -1e30
 MESH = pl.DeviceIdType.MESH
-ORDER = (2, 6, 1, 7)
+ORDER = (4, 2, 6, 1, 7)
 ARRIVE = (1, 7, 2, 6, 3, 5, 4)
-HALF = GRID_W // 2
-HAND = (
-    (2, 2, 4, (0, HALF), 4),
-    (2, 1, 3, (0, GRID_W), 3),
-    (6, -2, 4, (HALF, HALF), 0),
-    (6, -1, 5, (0, GRID_W), 5),
-)
+HAND = ((2, 1, 3), (6, -1, 5))
 
 
 def kernel(
@@ -290,17 +284,17 @@
             copy.wait_recv()
 
     def hand_on(array, row, coming, s_sems, r_sems):
-        for came, far, there, (first, size), sem in HAND:
+        spot = pl.ds(GRID_W * row, GRID_W)
+        for came, far, there in HAND:
             arrive(coming, came)
-            spot = pl.ds(GRID_W * row + first, size)
             copy = send(
                 array.at[came, spot, :],
                 array.at[there, spot, :],
-                s_sems.at[row, sem],
-                r_sems.at[row, sem],
+                s_sems.at[row, there],
+                r_sems.at[row, there],
                 peer(far),
             )
-            coming.setdefault(there, []).append(copy)
+            coming[there] = [copy]
 
     conditional = []
     x_gather = first_gather

time: 117 us -> 123 us (1.051)
  Pallas kernels: 116 us -> 121 us
    pallas_call x1, Pallas kernels: 116 us -> 121 us  [body(): pl.pallas_call(functools.partial(kernel, n_sp, n_tp, layers), out_shape=j...]
where the time goes in v9:
time: 123 us
  Pallas kernels  121 us (98%)
  local copies, waits for them, and re-layouts  1.47 us (1%)
    pallas_call x1, Pallas kernels, body(): pl.pallas_call(functools.partial(kernel, n_sp, n_tp, layers), out_shape=j...  121 us

profile of v9, /device:TPU:65, one launch (start us, length us, event | category | flops | bytes accessed | tf_op | source)
XLA Modules:
  0.0 122.6 jit_solution(4745091408961356512)
XLA Ops:
  0.0 121.1 %layers.1 = bf16[256,128]{1,0:T(8,128)(2,1)} custom-call(bf16[256,128]{1,0:T(8,128)(2,1)} %hid_ref.1, f32[3,2048]{1,0:T(4,128)} %gain_hbm.1, bf16[3,64,2048]{2,1,0:T(8,128)(2,1)} %wq_ref.1, bf16[3,64,2048]{2,1,0:T(8,128)(2,1)} %wk_ref.1, bf16[3,64,2048]{2,1,0:T(8,128)(2,1)} %wv_ref.1, bf16[3,1024,128]{2,1,0:T(8,128)(2,1)} %wo_ref.1, f32[3,15,1,31]{3,2,1,0:T(1,128)} %bitcast.1), custom_call_target="tpu_custom_call" | custom-call | tf_op jit(solution)/shard_map/layers/pallas_call | solution.py:468
  121.1 1.5 %copy.9 = bf16[256,128]{1,0:T(8,128)(2,1)} copy(bf16[256,128]{1,0:T(8,128)(2,1)} %layers.1) | data formatting | bytes 131072

commit v10 on v8

--- a/solution.py
+++ b/solution.py
@@ -65,8 +65,8 @@
     h_r,
 ):
     chips = n_tp // 2
-    tok = xs.shape[2]
-    feat = xs.shape[3]
+    tok = xs.shape[3]
+    feat = xs.shape[4]
     half = feat // 2
     tp = lax.axis_index("tp")
     sp = lax.axis_index("sp")
@@ -79,6 +79,10 @@
     def peer(j):
         return {"tp": lax.rem(tp + 2 * j + n_tp, n_tp)}
 
+    def place_of(j, owner):
+        at = owner if j in (1, chips - 1) else 1
+        return {"tp": 2 * lax.rem(chip + j, chips) + at}
+
     def rows_at(start, size, align):
         return pl.ds(pl.multiple_of(start, align), size)
 
@@ -93,7 +97,7 @@
     own_x = [
         pltpu.make_async_copy(hid_ref, xst, own_x_sem.at[0]),
         pltpu.make_async_copy(
-            hid_ref.at[rows_at(core * tok, tok, tok), :], xs.at[0, 0, :, my_lanes], own_x_sem.at[1]
+            hid_ref.at[rows_at(core * tok, tok, tok), :], xs.at[0, core, 0, :, my_lanes], own_x_sem.at[1]
         ),
     ]
     own_g = pltpu.make_async_copy(gain_hbm, gain_ref, own_x_sem.at[2])
@@ -150,20 +154,24 @@
         return copy
 
     own_x[0].wait()
-    first_gather = [{}, {}]
     for i in range(2):
         spot = pl.ds(GRID_W * i, GRID_W)
-        given = xst.at[rows_at((1 - core) * tok + GRID_W * i, GRID_W, GRID_W), :]
-        kept = xst.at[rows_at(core * tok + GRID_W * i, GRID_W, GRID_W), :]
-        for j in ORDER + (0,):
-            far = (2 * j + 1 - 2 * core + n_tp) if j else (1 - 2 * core + n_tp)
-            there = xs.at[0, j, spot, my_lanes]
-            pair = []
-            if j:
-                pair.append(send(kept, there, f_s.at[i, 0, j], f_r.at[i, 0, j], peer(j)))
-            device = {"tp": lax.rem(tp + far, n_tp)}
-            pair.append(send(given, there, f_s.at[i, 1, j], f_r.at[i, 1, j], device))
-            first_gather[i][j] = pair
+        for j in ORDER:
+            for owner in range(2):
+                send(
+                    xst.at[pl.ds(owner * tok + GRID_W * i, GRID_W), :],
+                    xs.at[0, owner, j, spot, my_lanes],
+                    f_s.at[owner, i, j],
+                    f_r.at[owner, i, core, j],
+                    place_of(j, owner),
+                )
+        send(
+            xst.at[rows_at((1 - core) * tok + GRID_W * i, GRID_W, GRID_W), :],
+            xs.at[0, 1 - core, 0, spot, my_lanes],
+            f_s.at[0, i, 0],
+            f_r.at[1 - core, i, core, 0],
+            {"tp": mate},
+        )
     t_mate = send(tab.at[0], tab.at[2], d2d_s.at[1], d2d_r.at[1], {"tp": mate})
     w_mate = []
     o_mate = []
@@ -285,31 +293,101 @@
             copies.append((copy, sent, got))
         return mine, copies
 
-    def arrive(coming, slot):
-        for copy in coming.pop(slot, ()):
-            copy.wait_recv()
-
-    def hand_on(array, row, coming, s_sems, r_sems):
-        for came, far, there, (first, size), sem in HAND:
-            arrive(coming, came)
-            spot = pl.ds(GRID_W * row + first, size)
-            copy = send(
-                array.at[came, spot, :],
-                array.at[there, spot, :],
-                s_sems.at[row, sem],
-                r_sems.at[row, sem],
-                peer(far),
+    def part_of(array, owner, slot, row, first=0, size=GRID_W):
+        return array.at[owner, slot, pl.ds(GRID_W * row + first, size), :]
+
+    def remote(src, dst, s_sem, r_sem, device):
+        return pltpu.make_async_remote_copy(
+            src_ref=src,
+            dst_ref=dst,
+            send_sem=s_sem,
+            recv_sem=r_sem,
+            device_id=device,
+            device_id_type=MESH,
+        )
+
+    def landed(there, sem):
+        remote(there, there, d2d_s.at[0], sem, {"tp": mate}).wait_recv()
+
+    def halves_landed(owner, slot, row, sources):
+        for source in sources:
+            lanes = rows_at(source * half, half, half)
+            landed(
+                xs.at[0, owner, slot, pl.ds(GRID_W * row, GRID_W), lanes],
+                f_r.at[owner, row, source, slot],
             )
-            coming.setdefault(there, []).append(copy)
+
+    def give(array, s_sems, r_sems, row):
+        for j in ORDER:
+            send(
+                part_of(array, core, 0, row),
+                part_of(array, core, j, row),
+                s_sems.at[0, row, j],
+                r_sems.at[core, row, j],
+                place_of(j, core),
+            )
+
+    def relay(array, s_sems, r_sems, row, owner, n):
+        came, far, there, (at, size), sem = HAND[n]
+        return remote(
+            part_of(array, owner, came, row, at, size),
+            part_of(array, owner, there, row, at, size),
+            s_sems.at[owner, row, 8 + n],
+            r_sems.at[owner, row, sem],
+            {"tp": 2 * lax.rem(chip + far + chips, chips) + owner},
+        )
+
+    def share(array, s_sems, r_sems, row, came):
+        own = part_of(array, 0, came, row)
+        return remote(
+            own, own, s_sems.at[0, row, 12 + came // 4], r_sems.at[0, row, came], {"tp": mate}
+        )
+
+    handed = []
+
+    def hand_on(array, s_sems, r_sems, row, first=False):
+        @pl.when(core == 1)
+        def _():
+            for owner in (1, 0):
+                for came in (2, 6):
+                    if first:
+                        halves_landed(owner, came, row, range(2))
+                    else:
+                        landed(part_of(array, owner, came, row), r_sems.at[owner, row, came])
+                    for n, hand in enumerate(HAND):
+                        if hand[0] == came:
+                            make = functools.partial(relay, array, s_sems, r_sems, row, owner, n)
+                            make().start()
+                            handed.append(make)
+                    if owner == 0:
+                        make = functools.partial(share, array, s_sems, r_sems, row, came)
+                        make().start()
+                        handed.append(make)
+
+    def arrive(array, r_sems, slot, row, first=False):
+        if slot == 0:
+            if first:
+                halves_landed(core, 0, row, (1 - core,))
+        elif slot in (2, 6):
+
+            @pl.when(core == 0)
+            def _():
+                landed(part_of(array, 0, slot, row), r_sems.at[0, row, slot])
+        elif slot == 4:
+            landed(part_of(array, core, 4, row, 0, HALF), r_sems.at[core, row, 4])
+            landed(part_of(array, core, 4, row, HALF, HALF), r_sems.at[core, row, 0])
+        elif first and slot in (1, 7):
+            halves_landed(core, slot, row, range(2))
+        else:
+            landed(part_of(array, core, slot, row), r_sems.at[core, row, slot])
 
     conditional = []
-    x_gather = first_gather
     for layer in range(layers):
         queries = []
         mates = []
         halos = []
         for i in range(2):
-            hand_on(xs.at[layer], i, x_gather[i], x_s.at[layer], x_r.at[layer])
+            hand_on(xs.at[layer], x_s.at[layer], x_r.at[layer], i, layer == 0)
         if layer == 0:
             own_g.wait()
             own_x[1].wait()
@@ -320,8 +398,8 @@
             made = None
             squares = None
             for j in (0,) + ARRIVE:
-                arrive(x_gather[i], j)
-                block = xs[layer, j, spot]
+                arrive(xs.at[layer], x_r.at[layer], j, i, layer == 0)
+                block = xs[layer, core, j, spot]
                 wide = block.astype(jnp.float32)
                 square = wide * wide
                 part = lax.dot_general(
@@ -354,8 +432,6 @@
             def _(copy=copy):
                 copy.wait_recv()
 
-        gather = [{}, {}]
-        x_gather = [{}, {}]
         for i in range(2):
             spot = pl.ds(GRID_W * i, GRID_W)
             outs = []
@@ -379,20 +455,12 @@
                 )
                 outs.append(mixed / total)
             both = jnp.where(lane_low, outs[0], outs[1])
-            atts[layer, 0, spot, :] = both.astype(jnp.bfloat16)
-            for j in ORDER:
-                copy = send(
-                    atts.at[layer, 0, spot, :],
-                    atts.at[layer, j, spot, :],
-                    a_s.at[layer, i, j],
-                    a_r.at[layer, i, j],
-                    peer(j),
-                )
-                gather[i][j] = [copy]
+            atts[layer, core, 0, spot, :] = both.astype(jnp.bfloat16)
+            give(atts.at[layer], a_s.at[layer], a_r.at[layer], i)
         before = list(sends[: -2 * len(ORDER)])
         del sends[: len(before)]
         for i in range(2):
-            hand_on(atts.at[layer], i, gather[i], a_s.at[layer], a_r.at[layer])
+            hand_on(atts.at[layer], a_s.at[layer], a_r.at[layer], i)
         if layer + 1 < layers:
             give_weights(layer + 1)
         for copy in before:
@@ -404,27 +472,19 @@
         kept = []
         for i in range(2):
             spot = pl.ds(GRID_W * i, GRID_W)
-            stream = xs[layer, 0, spot].astype(jnp.float32)
+            stream = xs[layer, core, 0, spot].astype(jnp.float32)
             for j in (0,) + ARRIVE:
-                arrive(gather[i], j)
+                arrive(atts.at[layer], a_r.at[layer], j, i)
                 source = lax.rem(chip - j + chips, chips)
                 stream = stream + jnp.dot(
-                    atts[layer, j, spot],
+                    atts[layer, core, j, spot],
                     wout[layer, rows_at(source * 128, 128, 128), :],
                     preferred_element_type=jnp.float32,
                 )
             final = stream.astype(jnp.bfloat16)
             if layer + 1 < layers:
-                xs[layer + 1, 0, spot, :] = final
-                for j in ORDER:
-                    copy = send(
-                        xs.at[layer + 1, 0, spot, :],
-                        xs.at[layer + 1, j, spot, :],
-                        x_s.at[layer + 1, i, j],
-                        x_r.at[layer + 1, i, j],
-                        peer(j),
-                    )
-                    x_gather[i][j] = [copy]
+                xs[layer + 1, core, 0, spot, :] = final
+                give(xs.at[layer + 1], x_s.at[layer + 1], x_r.at[layer + 1], i)
             else:
                 swap = core == 0
                 last_half[spot, :] = jnp.where(swap, final[:, half:feat], final[:, 0:half])
@@ -456,6 +516,11 @@
 
     for copy in sends:
         copy.wait_send()
+
+    @pl.when(core == 1)
+    def _():
+        for make in handed:
+            make().wait_send()
 
 
 def body(hidden_in, norm_gain, query_weight, key_weight, value_weight, output_weight, offset_bias):
@@ -482,8 +547,8 @@
             pltpu.VMEM((tokens, feat // 2), bf16),
             pltpu.VMEM((tok, feat // 2), bf16),
             pltpu.VMEM((tok, feat // 2), bf16),
-            pltpu.VMEM((layers, chips, tok, feat), bf16),
-            pltpu.VMEM((layers, chips, tok, 128), bf16),
+            pltpu.VMEM((layers, 2, chips, tok, feat), bf16),
+            pltpu.VMEM((layers, 2, chips, tok, 128), bf16),
             pltpu.VMEM((layers, 768, 256), bf16),
             pltpu.VMEM((layers, 384, width), bf16),
             pltpu.VMEM((layers, chips, 384, feat), bf16),
@@ -496,11 +561,11 @@
             dma((4 + 4 * layers,)),
             dma((4 + 4 * layers,)),
             dma((2, 2, chips)),
-            dma((2, 2, chips)),
-            dma((layers, 2, chips)),
-            dma((layers, 2, chips)),
-            dma((layers, 2, chips)),
-            dma((layers, 2, chips)),
+            dma((2, 2, 2, chips)),
+            dma((layers, 2, 2, 16)),
+            dma((layers, 2, 2, chips)),
+            dma((layers, 2, 2, 16)),
+            dma((layers, 2, 2, chips)),
             dma((layers, 2, 5)),
             dma((layers, 2, 5)),
         ],

time: 117 us -> 118 us (level)
  no operation moved by 1% of the time
where the time goes in v10:
time: 118 us
  Pallas kernels  116 us (98%)
  local copies, waits for them, and re-layouts  1.47 us (1%)
    pallas_call x1, Pallas kernels, body(): pl.pallas_call(functools.partial(kernel, n_sp, n_tp, layers), out_shape=j...  116 us

profile of v10, /device:TPU:65, one launch (start us, length us, event | category | flops | bytes accessed | tf_op | source)
XLA Modules:
  0.0 117.6 jit_solution(15008141203599723991)
XLA Ops:
  0.0 116.1 %layers.1 = bf16[256,128]{1,0:T(8,128)(2,1)} custom-call(bf16[256,128]{1,0:T(8,128)(2,1)} %hid_ref.1, f32[3,2048]{1,0:T(4,128)} %gain_hbm.1, bf16[3,64,2048]{2,1,0:T(8,128)(2,1)} %wq_ref.1, bf16[3,64,2048]{2,1,0:T(8,128)(2,1)} %wk_ref.1, bf16[3,64,2048]{2,1,0:T(8,128)(2,1)} %wv_ref.1, bf16[3,1024,128]{2,1,0:T(8,128)(2,1)} %wo_ref.1, f32[3,15,1,31]{3,2,1,0:T(1,128)} %bitcast.1), custom_call_target="tpu_custom_call" | custom-call | tf_op jit(solution)/shard_map/layers/pallas_call | solution.py:539
  116.1 1.5 %copy.9 = bf16[256,128]{1,0:T(8,128)(2,1)} copy(bf16[256,128]{1,0:T(8,128)(2,1)} %layers.1) | data formatting | bytes 131072

commit v11 on v9

--- a/solution.py
+++ b/solution.py
@@ -14,9 +14,14 @@
 EPS = 1e-06
 NEG = -1e30
 MESH = pl.DeviceIdType.MESH
-ORDER = (4, 2, 6, 1, 7)
+ORDER = (2, 6, 1, 7)
 ARRIVE = (1, 7, 2, 6, 3, 5, 4)
-HAND = ((2, 1, 3), (6, -1, 5))
+HALF = GRID_W // 2
+WHOLE = (0, GRID_W)
+STAGES = (
+    ((2, 1, 3, WHOLE, 3), (6, -1, 5, WHOLE, 5)),
+    ((3, 1, 4, (0, HALF), 4), (5, -1, 4, (HALF, HALF), 0)),
+)
 
 
 def kernel(
@@ -283,18 +288,20 @@
         for copy in coming.pop(slot, ()):
             copy.wait_recv()
 
-    def hand_on(array, row, coming, s_sems, r_sems):
-        spot = pl.ds(GRID_W * row, GRID_W)
-        for came, far, there in HAND:
-            arrive(coming, came)
-            copy = send(
-                array.at[came, spot, :],
-                array.at[there, spot, :],
-                s_sems.at[row, there],
-                r_sems.at[row, there],
-                peer(far),
-            )
-            coming[there] = [copy]
+    def hand_on(array, coming, s_sems, r_sems):
+        for stage in STAGES:
+            for row in range(2):
+                for came, far, there, (first, size), sem in stage:
+                    arrive(coming[row], came)
+                    spot = pl.ds(GRID_W * row + first, size)
+                    copy = send(
+                        array.at[came, spot, :],
+                        array.at[there, spot, :],
+                        s_sems.at[row, sem],
+                        r_sems.at[row, sem],
+                        peer(far),
+                    )
+                    coming[row].setdefault(there, []).append(copy)
 
     conditional = []
     x_gather = first_gather
@@ -302,8 +309,7 @@
         queries = []
         mates = []
         halos = []
-        for i in range(2):
-            hand_on(xs.at[layer], i, x_gather[i], x_s.at[layer], x_r.at[layer])
+        hand_on(xs.at[layer], x_gather, x_s.at[layer], x_r.at[layer])
         if layer == 0:
             own_g.wait()
             own_x[1].wait()
@@ -385,8 +391,7 @@
                 gather[i][j] = [copy]
         before = list(sends[: -2 * len(ORDER)])
         del sends[: len(before)]
-        for i in range(2):
-            hand_on(atts.at[layer], i, gather[i], a_s.at[layer], a_r.at[layer])
+        hand_on(atts.at[layer], gather, a_s.at[layer], a_r.at[layer])
         if layer + 1 < layers:
             give_weights(layer + 1)
         for copy in before:

time: 123 us -> 129 us (1.049)
  Pallas kernels: 121 us -> 128 us
    pallas_call x1, Pallas kernels: 121 us -> 128 us  [body(): pl.pallas_call(functools.partial(kernel, n_sp, n_tp, layers), out_shape=j...]
where the time goes in v11:
time: 129 us
  Pallas kernels  128 us (99%)
  local copies, waits for them, and re-layouts  1.47 us (1%)
    pallas_call x1, Pallas kernels, body(): pl.pallas_call(functools.partial(kernel, n_sp, n_tp, layers), out_shape=j...  128 us

profile of v11, /device:TPU:65, one launch (start us, length us, event | category | flops | bytes accessed | tf_op | source)
XLA Modules:
  0.0 129.3 jit_solution(11909375068466955778)
XLA Ops:
  0.0 127.8 %layers.1 = bf16[256,128]{1,0:T(8,128)(2,1)} custom-call(bf16[256,128]{1,0:T(8,128)(2,1)} %hid_ref.1, f32[3,2048]{1,0:T(4,128)} %gain_hbm.1, bf16[3,64,2048]{2,1,0:T(8,128)(2,1)} %wq_ref.1, bf16[3,64,2048]{2,1,0:T(8,128)(2,1)} %wk_ref.1, bf16[3,64,2048]{2,1,0:T(8,128)(2,1)} %wv_ref.1, bf16[3,1024,128]{2,1,0:T(8,128)(2,1)} %wo_ref.1, f32[3,15,1,31]{3,2,1,0:T(1,128)} %bitcast.1), custom_call_target="tpu_custom_call" | custom-call | tf_op jit(solution)/shard_map/layers/pallas_call | solution.py:473
  127.8 1.5 %copy.9 = bf16[256,128]{1,0:T(8,128)(2,1)} copy(bf16[256,128]{1,0:T(8,128)(2,1)} %layers.1) | data formatting | bytes 131072

commit v12 on v8

--- a/solution.py
+++ b/solution.py
@@ -356,30 +356,36 @@
 
         gather = [{}, {}]
         x_gather = [{}, {}]
+        cases = [(i, head) for i in range(2) for head in range(2)]
+        pairs = [
+            kv[
+                layer,
+                rows_at(starts[i] * GRID_W, ROW_SPAN * GRID_W, GRID_W),
+                128 * head : 128 * head + 128,
+            ]
+            for i, head in cases
+        ]
+        scores = []
+        for (i, head), pair in zip(cases, pairs, strict=True):
+            pick = lane_low if head == 1 else jnp.logical_not(lane_low)
+            query = jnp.where(pick, queries[i], 0)
+            score = lax.dot_general(
+                query, pair, (((1,), (1,)), ((), ())), preferred_element_type=jnp.float32
+            )
+            scores.append(score + bias[layer, head, i])
+        peaks = [jnp.max(score, axis=1, keepdims=True) for score in scores]
+        lifted = [jnp.exp(score - peak) for score, peak in zip(scores, peaks, strict=True)]
+        totals = [jnp.sum(lift, axis=1, keepdims=True) for lift in lifted]
+        mixed = [
+            jnp.dot(lift.astype(jnp.bfloat16), pair, preferred_element_type=jnp.float32)
+            for lift, pair in zip(lifted, pairs, strict=True)
+        ]
+        outs = [mix / total for mix, total in zip(mixed, totals, strict=True)]
+        for i in range(2):
+            both = jnp.where(lane_low, outs[2 * i], outs[2 * i + 1])
+            atts[layer, 0, GRID_W * i : GRID_W * (i + 1), :] = both.astype(jnp.bfloat16)
         for i in range(2):
             spot = pl.ds(GRID_W * i, GRID_W)
-            outs = []
-            for head in range(2):
-                pick = lane_low if head == 1 else jnp.logical_not(lane_low)
-                query = jnp.where(pick, queries[i], 0)
-                pairs = kv[
-                    layer,
-                    rows_at(starts[i] * GRID_W, ROW_SPAN * GRID_W, GRID_W),
-                    128 * head : 128 * head + 128,
-                ]
-                scores = lax.dot_general(
-                    query, pairs, (((1,), (1,)), ((), ())), preferred_element_type=jnp.float32
-                )
-                scores = scores + bias[layer, head, i]
-                peak = jnp.max(scores, axis=1, keepdims=True)
-                lifted = jnp.exp(scores - peak)
-                total = jnp.sum(lifted, axis=1, keepdims=True)
-                mixed = jnp.dot(
-                    lifted.astype(jnp.bfloat16), pairs, preferred_element_type=jnp.float32
-                )
-                outs.append(mixed / total)
-            both = jnp.where(lane_low, outs[0], outs[1])
-            atts[layer, 0, spot, :] = both.astype(jnp.bfloat16)
             for j in ORDER:
                 copy = send(
                     atts.at[layer, 0, spot, :],

time: 117 us -> 117 us (level)
  no operation moved by 1% of the time
where the time goes in v12:
time: 117 us
  Pallas kernels  116 us (99%)
  local copies, waits for them, and re-layouts  1.47 us (1%)
    pallas_call x1, Pallas kernels, body(): pl.pallas_call(functools.partial(kernel, n_sp, n_tp, layers), out_shape=j...  116 us

profile of v12, /device:TPU:65, one launch (start us, length us, event | category | flops | bytes accessed | tf_op | source)
XLA Modules:
  0.0 117.2 jit_solution(5342419468506244721)
XLA Ops:
  0.0 115.7 %layers.1 = bf16[256,128]{1,0:T(8,128)(2,1)} custom-call(bf16[256,128]{1,0:T(8,128)(2,1)} %hid_ref.1, f32[3,2048]{1,0:T(4,128)} %gain_hbm.1, bf16[3,64,2048]{2,1,0:T(8,128)(2,1)} %wq_ref.1, bf16[3,64,2048]{2,1,0:T(8,128)(2,1)} %wk_ref.1, bf16[3,64,2048]{2,1,0:T(8,128)(2,1)} %wv_ref.1, bf16[3,1024,128]{2,1,0:T(8,128)(2,1)} %wo_ref.1, f32[3,15,1,31]{3,2,1,0:T(1,128)} %bitcast.1), custom_call_target="tpu_custom_call" | custom-call | tf_op jit(solution)/shard_map/layers/pallas_call | solution.py:480
  115.7 1.5 %copy.9 = bf16[256,128]{1,0:T(8,128)(2,1)} copy(bf16[256,128]{1,0:T(8,128)(2,1)} %layers.1) | data formatting | bytes 131072

commit v13 on v12

--- a/solution.py
+++ b/solution.py
@@ -15,6 +15,7 @@
 NEG = -1e30
 MESH = pl.DeviceIdType.MESH
 ORDER = (2, 6, 1, 7)
+QUEUE = ((0, 2), (0, 6), (1, 2), (1, 6), (0, 1), (0, 7), (1, 1), (1, 7))
 ARRIVE = (1, 7, 2, 6, 3, 5, 4)
 HALF = GRID_W // 2
 HAND = (
@@ -151,19 +152,18 @@
 
     own_x[0].wait()
     first_gather = [{}, {}]
-    for i in range(2):
+    for i, j in QUEUE + ((0, 0), (1, 0)):
         spot = pl.ds(GRID_W * i, GRID_W)
         given = xst.at[rows_at((1 - core) * tok + GRID_W * i, GRID_W, GRID_W), :]
         kept = xst.at[rows_at(core * tok + GRID_W * i, GRID_W, GRID_W), :]
-        for j in ORDER + (0,):
-            far = (2 * j + 1 - 2 * core + n_tp) if j else (1 - 2 * core + n_tp)
-            there = xs.at[0, j, spot, my_lanes]
-            pair = []
-            if j:
-                pair.append(send(kept, there, f_s.at[i, 0, j], f_r.at[i, 0, j], peer(j)))
-            device = {"tp": lax.rem(tp + far, n_tp)}
-            pair.append(send(given, there, f_s.at[i, 1, j], f_r.at[i, 1, j], device))
-            first_gather[i][j] = pair
+        far = (2 * j + 1 - 2 * core + n_tp) if j else (1 - 2 * core + n_tp)
+        there = xs.at[0, j, spot, my_lanes]
+        pair = []
+        if j:
+            pair.append(send(kept, there, f_s.at[i, 0, j], f_r.at[i, 0, j], peer(j)))
+        device = {"tp": lax.rem(tp + far, n_tp)}
+        pair.append(send(given, there, f_s.at[i, 1, j], f_r.at[i, 1, j], device))
+        first_gather[i][j] = pair
     t_mate = send(tab.at[0], tab.at[2], d2d_s.at[1], d2d_r.at[1], {"tp": mate})
     w_mate = []
     o_mate = []
@@ -384,17 +384,16 @@
         for i in range(2):
             both = jnp.where(lane_low, outs[2 * i], outs[2 * i + 1])
             atts[layer, 0, GRID_W * i : GRID_W * (i + 1), :] = both.astype(jnp.bfloat16)
-        for i in range(2):
+        for i, j in QUEUE:
             spot = pl.ds(GRID_W * i, GRID_W)
-            for j in ORDER:
-                copy = send(
-                    atts.at[layer, 0, spot, :],
-                    atts.at[layer, j, spot, :],
-                    a_s.at[layer, i, j],
-                    a_r.at[layer, i, j],
-                    peer(j),
-                )
-                gather[i][j] = [copy]
+            copy = send(
+                atts.at[layer, 0, spot, :],
+                atts.at[layer, j, spot, :],
+                a_s.at[layer, i, j],
+                a_r.at[layer, i, j],
+                peer(j),
+            )
+            gather[i][j] = [copy]
         before = list(sends[: -2 * len(ORDER)])
         del sends[: len(before)]
         for i in range(2):

time: 117 us -> 117 us (level)
  no operation moved by 1% of the time
where the time goes in v13:
time: 117 us; the launch traced here: 116 us
  Pallas kernels  115 us (98%)
  local copies, waits for them, and re-layouts  1.47 us (1%)
    pallas_call x1, Pallas kernels, body(): pl.pallas_call(functools.partial(kernel, n_sp, n_tp, layers), out_shape=j...  115 us

profile of v13, /device:TPU:65, one launch (start us, length us, event | category | flops | bytes accessed | tf_op | source)
XLA Modules:
  0.0 116.5 jit_solution(117204142964068512)
XLA Ops:
  0.0 115.0 %layers.1 = bf16[256,128]{1,0:T(8,128)(2,1)} custom-call(bf16[256,128]{1,0:T(8,128)(2,1)} %hid_ref.1, f32[3,2048]{1,0:T(4,128)} %gain_hbm.1, bf16[3,64,2048]{2,1,0:T(8,128)(2,1)} %wq_ref.1, bf16[3,64,2048]{2,1,0:T(8,128)(2,1)} %wk_ref.1, bf16[3,64,2048]{2,1,0:T(8,128)(2,1)} %wv_ref.1, bf16[3,1024,128]{2,1,0:T(8,128)(2,1)} %wo_ref.1, f32[3,15,1,31]{3,2,1,0:T(1,128)} %bitcast.1), custom_call_target="tpu_custom_call" | custom-call | tf_op jit(solution)/shard_map/layers/pallas_call | solution.py:479
  115.0 1.5 %copy.9 = bf16[256,128]{1,0:T(8,128)(2,1)} copy(bf16[256,128]{1,0:T(8,128)(2,1)} %layers.1) | data formatting | bytes 131072

commit v14 on v13

--- a/solution.py
+++ b/solution.py
@@ -449,10 +449,6 @@
                 )
                 copy.start()
                 kept.append(copy)
-        for copy in last:
-            copy.wait_recv()
-        for copy in kept:
-            copy.wait()
     for copy, sent, _ in conditional:
 
         @pl.when(sent)
@@ -461,6 +457,10 @@
 
     for copy in sends:
         copy.wait_send()
+    for copy in last:
+        copy.wait_recv()
+    for copy in kept:
+        copy.wait()
 
 
 def body(hidden_in, norm_gain, query_weight, key_weight, value_weight, output_weight, offset_bias):

time: 117 us -> 117 us (level)
  no operation moved by 1% of the time
where the time goes in v14:
time: 117 us; the launch traced here: 116 us
  Pallas kernels  115 us (98%)
  local copies, waits for them, and re-layouts  1.47 us (1%)
    pallas_call x1, Pallas kernels, body(): pl.pallas_call(functools.partial(kernel, n_sp, n_tp, layers), out_shape=j...  115 us

profile of v14, /device:TPU:65, one launch (start us, length us, event | category | flops | bytes accessed | tf_op | source)
XLA Modules:
  0.0 116.4 jit_solution(15720277550671339995)
XLA Ops:
  0.0 114.9 %layers.1 = bf16[256,128]{1,0:T(8,128)(2,1)} custom-call(bf16[256,128]{1,0:T(8,128)(2,1)} %hid_ref.1, f32[3,2048]{1,0:T(4,128)} %gain_hbm.1, bf16[3,64,2048]{2,1,0:T(8,128)(2,1)} %wq_ref.1, bf16[3,64,2048]{2,1,0:T(8,128)(2,1)} %wk_ref.1, bf16[3,64,2048]{2,1,0:T(8,128)(2,1)} %wv_ref.1, bf16[3,1024,128]{2,1,0:T(8,128)(2,1)} %wo_ref.1, f32[3,15,1,31]{3,2,1,0:T(1,128)} %bitcast.1), custom_call_target="tpu_custom_call" | custom-call | tf_op jit(solution)/shard_map/layers/pallas_call | solution.py:479
  114.9 1.5 %copy.9 = bf16[256,128]{1,0:T(8,128)(2,1)} copy(bf16[256,128]{1,0:T(8,128)(2,1)} %layers.1) | data formatting | bytes 131072
